TPU v7x, 32 devices: a whole 2x2x4 slice. The times are simulated.
32 devices in a mesh: dp: 2 (over x), kv: 8 (over z, y), tp: 2 (over core).
Axes of the slice: x: 2, y: 2, z: 4, core: 2. Of those that a mesh axis runs over, the one named last changes fastest.
Arguments:
- tokens: bfloat16 [32, 3072], P(('tp', 'dp'), 'kv'), parts along dimension 0, may hold values from -60 to 60
- old_state: float32 [32, 24, 128, 128], P(('tp', 'dp', 'kv')), parts along dimension 0, may hold values from -0.6 to 0.6
- mixer_gain: float32 [3072], replicated, may hold values from 0.1 to 1.9
- w_query: bfloat16 [3072, 3072], P(None, 'kv'), may hold values from -0.109375 to 0.109375
- w_key: bfloat16 [3072, 3072], P(None, 'kv'), may hold values from -0.109375 to 0.109375
- w_value: bfloat16 [3072, 3072], P(None, 'kv'), may hold values from -0.109375 to 0.109375
- w_outgate: bfloat16 [3072, 3072], P(None, 'kv'), may hold values from -0.109375 to 0.109375
- w_decay: bfloat16 [3072, 24], replicated, may hold values from -0.109375 to 0.109375
- w_write: bfloat16 [3072, 24], replicated, may hold values from -0.109375 to 0.109375
- decay_log: float32 [24], replicated, may hold values from -3 to 1
- decay_bias: float32 [24], replicated, may hold values from -3 to 3
- head_gain: float32 [128], replicated, may hold values from 0.1 to 1.9
- w_output: bfloat16 [3072, 3072], P('kv'), may hold values from -0.15625 to 0.15625
- channel_gain: float32 [3072], replicated, may hold values from 0.1 to 1.9
- w_gate: bfloat16 [3072, 8448], P(None, 'kv'), may hold values from -0.109375 to 0.109375
- w_up: bfloat16 [3072, 8448], P(None, 'kv'), may hold values from -0.109375 to 0.109375
- w_down: bfloat16 [8448, 3072], P(None, 'kv'), may hold values from -0.0625 to 0.0625
Outputs:
- mixed: bfloat16 [32, 3072], P(('tp', 'dp'), 'kv'), parts along dimension 0
- new_state: float32 [32, 24, 128, 128], P(('tp', 'dp', 'kv')), parts along dimension 0
There are 2 independent parts, one for each index of `tp`. A program takes and returns all parts, laid end to end along the dimension named above; an argument that names none is the same for every part. Nothing has to cross between parts.
All inputs are finite; a program needn't handle non-finite values.
Results may differ from a plain program's by a relative error of at most 0.0059.
Values may be sent and summed in bfloat16 or wider, within the bound.
No kernel may reach another device: no remote copies, remote signals or barrier semaphores. Data moves between devices by JAX's collectives and lax.ppermute only.
A program may use at most 64 MiB of HBM per device.

v0:
```python
import jax
import jax.numpy as jnp
from jax import lax
from jax.sharding import PartitionSpec as P

HEADS = 24
HEAD_DIM = 128


EPS = 1e-06


def norm_scale(values):
    return lax.rsqrt(jnp.mean(values * values, axis=-1, keepdims=True) + EPS)


def unit_rows(values):
    return values * lax.rsqrt(jnp.sum(values * values, axis=-1, keepdims=True) + EPS)


def body(
    tokens,
    old_state,
    mixer_gain,
    w_query,
    w_key,
    w_value,
    w_outgate,
    w_decay,
    w_write,
    decay_log,
    decay_bias,
    head_gain,
    w_output,
    channel_gain,
    w_gate,
    w_up,
    w_down,
):
    local_rows = old_state.shape[0]
    width_share = tokens.shape[1]
    offset_rows = lax.axis_index("kv") * local_rows
    offset_cols = lax.axis_index("kv") * width_share
    complete_rows = lax.all_gather(tokens, "kv", axis=1, tiled=True)
    tok_wide = complete_rows.astype(jnp.float32)
    scale_in = norm_scale(tok_wide)
    normed = (tok_wide * mixer_gain).astype(jnp.bfloat16)

    def project(weight):
        return (jnp.dot(normed, weight, preferred_element_type=jnp.float32) * scale_in).astype(
            jnp.bfloat16
        )

    query_cols = project(w_query)
    key_cols = project(w_key)
    value_cols = project(w_value)
    outgate_cols = project(w_outgate)
    query_pre, key_pre, value_pre, outgate_pre = (
        lax.all_to_all(query_cols, "kv", split_axis=0, concat_axis=1, tiled=True),
        lax.all_to_all(key_cols, "kv", split_axis=0, concat_axis=1, tiled=True),
        lax.all_to_all(value_cols, "kv", split_axis=0, concat_axis=1, tiled=True),
        lax.all_to_all(outgate_cols, "kv", split_axis=0, concat_axis=1, tiled=True),
    )
    own_normed = lax.dynamic_slice_in_dim(normed, offset_rows, local_rows, 0)
    own_scale = lax.dynamic_slice_in_dim(scale_in, offset_rows, local_rows, 0)
    decay_pre = jnp.dot(own_normed, w_decay, preferred_element_type=jnp.float32) * own_scale
    write_pre = jnp.dot(own_normed, w_write, preferred_element_type=jnp.float32) * own_scale

    def by_head(values):
        return values.astype(jnp.float32).reshape(local_rows, HEADS, HEAD_DIM)

    queries = unit_rows(jax.nn.silu(by_head(query_pre))) * HEAD_DIM ** (-0.5)
    keys_unit = unit_rows(jax.nn.silu(by_head(key_pre)))
    values_act = jax.nn.silu(by_head(value_pre))
    strength = jax.nn.sigmoid(write_pre)
    retain = jnp.exp(-jnp.exp(decay_log) * jax.nn.softplus(decay_pre + decay_bias))
    recalled_values = jnp.einsum(
        "bhkv,bhk->bhv", old_state, keys_unit, precision=lax.Precision.HIGHEST
    )
    correction = values_act - retain[..., None] * recalled_values
    new_state = (
        retain[..., None, None] * old_state
        + (strength[..., None] * keys_unit)[..., :, None] * correction[..., None, :]
    )
    state_readout = jnp.einsum("bhkv,bhk->bhv", new_state, queries, precision=lax.Precision.HIGHEST)
    gated_read = (
        state_readout * norm_scale(state_readout) * head_gain * jax.nn.silu(by_head(outgate_pre))
    )
    gated_read = gated_read.reshape(local_rows, HEADS * HEAD_DIM).astype(jnp.bfloat16)
    read_cols = lax.all_to_all(gated_read, "kv", split_axis=1, concat_axis=0, tiled=True)
    partial_out = jnp.dot(read_cols, w_output, preferred_element_type=jnp.float32)
    mixer_out = lax.psum(partial_out, "kv")
    residual = lax.optimization_barrier((tok_wide + mixer_out).astype(jnp.bfloat16))
    residual_wide = residual.astype(jnp.float32)
    scale_mid = norm_scale(residual_wide)
    normed_mid = (residual_wide * channel_gain).astype(jnp.bfloat16)
    gate_act = jnp.dot(normed_mid, w_gate, preferred_element_type=jnp.float32) * scale_mid
    upward = jnp.dot(normed_mid, w_up, preferred_element_type=jnp.float32) * scale_mid
    own_residual = lax.dynamic_slice_in_dim(residual_wide, offset_cols, width_share, 1)
    hidden_units = (jax.nn.silu(gate_act) * upward).astype(jnp.bfloat16)
    down_sum = jnp.dot(
        lax.all_gather(hidden_units, "kv", axis=1, tiled=True),
        w_down,
        preferred_element_type=jnp.float32,
    )
    mixed = (own_residual + down_sum).astype(jnp.bfloat16)
    return (mixed, new_state)


def solution(mesh):
    in_specs = (
        P(("tp", "dp"), "kv"),
        P(("tp", "dp", "kv"), None, None, None),
        P(),
        P(None, "kv"),
        P(None, "kv"),
        P(None, "kv"),
        P(None, "kv"),
        P(),
        P(),
        P(),
        P(),
        P(),
        P("kv", None),
        P(),
        P(None, "kv"),
        P(None, "kv"),
        P(None, "kv"),
    )
    out_specs = (P(("tp", "dp"), "kv"), P(("tp", "dp", "kv"), None, None, None))
    return jax.shard_map(body, mesh=mesh, in_specs=in_specs, out_specs=out_specs, check_vma=False)
```

profile of v0, /device:TPU:0, one launch (start us, length us, event | category | flops | bytes accessed | tf_op | source)
XLA Modules:
  0.0 226.5 jit_solution(14168076446692269067)
XLA Ops:
  7.2 32.9 %all_gather.6 = bf16[8,3072]{1,0:T(8,128)(2,1)S(1)} all-gather(bf16[8,384]{1,0:T(8,128)(2,1)} %param.17), channel_id=1, replica_groups=mesh['dp'=2,'kv'=8,'tp'=2] {'kv'}, dimensions={1}, use_global_device_ids=true | all-gather | bytes 55296 | tf_op jit(solution)/shard_map/all_gather | solution.py:44
  40.1 0.8 fusion.24
  41.0 2.1 fusion.15
  43.0 0.5 broadcast.215
  43.6 0.6 reduce.6
  44.2 0.7 reshape.400
  44.9 5.4 %all-to-all-start = ((bf16[8,2,192]{2,1,0:T(2,128)(2,1)}), bf16[8,2,192]{2,1,0:T(2,128)(2,1)S(1)}, u32[]{:S(2)}, u32[]{:S(2)}) async-start(bf16[8,2,192]{2,1,0:T(2,128)(2,1)} %reshape.400), calls=%async_computation | async-start | bytes 16384 | tf_op jit(solution)/shard_map/all_to_all | solution.py:60
  50.3 0.6 dynamic-slice.3
  50.9 2.2 fusion.14
  53.1 0.4 fusion.13
  53.6 0.4 fusion.12
  54.0 0.1 copy-done.5
  54.1 0.8 fusion.46
  54.9 0.8 fusion.20
  55.7 0.7 reduce.7
  56.4 0.7 reshape.402
  57.1 0.6 reduce.5
  57.8 0.7 reshape.398
  58.4 0.6 reduce.4
  59.1 0.7 reshape.396
  59.8 6.0 %all-to-all-start.1 = ((bf16[8,2,192]{2,1,0:T(2,128)(2,1)}), bf16[8,2,192]{2,1,0:T(2,128)(2,1)S(1)}, u32[]{:S(2)}, u32[]{:S(2)}) async-start(bf16[8,2,192]{2,1,0:T(2,128)(2,1)} %reshape.402), calls=%async_computation.1 | async-start | bytes 16384 | tf_op jit(solution)/shard_map/all_to_all | solution.py:61
  65.8 0.1 reshape.401
  65.9 0.1 fusion.36
  66.0 6.3 %all-to-all-done.1 = bf16[8,2,192]{2,1,0:T(2,128)(2,1)S(1)} async-done(((bf16[8,2,192]{2,1,0:T(2,128)(2,1)}), bf16[8,2,192]{2,1,0:T(2,128)(2,1)S(1)}, u32[]{:S(2)}, u32[]{:S(2)}) %all-to-all-start.1) | async-done | bytes 6176 | tf_op jit(solution)/shard_map/all_to_all | solution.py:61
  72.3 3.3 %all-to-all-start.2 = ((bf16[8,2,192]{2,1,0:T(2,128)(2,1)}), bf16[8,2,192]{2,1,0:T(2,128)(2,1)S(1)}, u32[]{:S(2)}, u32[]{:S(2)}) async-start(bf16[8,2,192]{2,1,0:T(2,128)(2,1)} %reshape.398), calls=%async_computation.2 | async-start | bytes 16384 | tf_op jit(solution)/shard_map/all_to_all | solution.py:59
  75.6 0.1 reshape.403
  75.8 6.3 %all-to-all-done.2 = bf16[8,2,192]{2,1,0:T(2,128)(2,1)S(1)} async-done(((bf16[8,2,192]{2,1,0:T(2,128)(2,1)}), bf16[8,2,192]{2,1,0:T(2,128)(2,1)S(1)}, u32[]{:S(2)}, u32[]{:S(2)}) %all-to-all-start.2) | async-done | bytes 6176 | tf_op jit(solution)/shard_map/all_to_all | solution.py:59
  82.1 3.3 %all-to-all-start.3 = ((bf16[8,2,192]{2,1,0:T(2,128)(2,1)}), bf16[8,2,192]{2,1,0:T(2,128)(2,1)S(1)}, u32[]{:S(2)}, u32[]{:S(2)}) async-start(bf16[8,2,192]{2,1,0:T(2,128)(2,1)} %reshape.396), calls=%async_computation.3 | async-start | bytes 16384 | tf_op jit(solution)/shard_map/all_to_all | solution.py:62
  85.5 0.1 reshape.399
  85.6 0.1 fusion.37
  85.8 2.9 %fusion.5 = f32[24,1,128]{2,1,0:T(1,128)S(1)} fusion(f32[24,128,1]{1,2,0:T(1,128)S(1)} %bitcast.127, f32[1,24,128,128]{3,2,1,0:T(8,128)} %param.18), kind=kOutput, calls=%fused_computation.7 | convolution fusion | flops 4718592 | bytes 1597440 | tf_op jit(solution)/shard_map/bhkv,bhk->bhv/dot_general | solution.py:77
  88.8 0.6 multiply_add_fusion
  89.5 1.1 copy-done.2
  90.5 1.4 fusion.3
  92.0 0.1 multiply_reduce_fusion.1
  92.1 0.1 reshape.397
  92.3 0.7 reduce.8
  93.1 12.2 %all_to_all.65 = bf16[8,2,192]{2,1,0:T(2,128)(2,1)S(1)} all-to-all(bf16[8,2,192]{2,1,0:T(2,128)(2,1)S(1)} %reshape.404), channel_id=1, replica_groups=mesh['dp'=2,'kv'=8,'tp'=2] {'kv'}, dimensions={0} | all-to-all | bytes 12288 | tf_op jit(solution)/shard_map/all_to_all | solution.py:90
  105.3 0.1 reshape.405
  105.4 1.1 fusion.40
  106.5 67.6 %all-reduce.2.cloned.1.call-done = f32[8,3072]{1,0:T(8,128)} async-done(((f32[8,3072]{1,0:T(8,128)}), f32[8,3072]{1,0:T(8,128)}) %all-reduce.2.cloned.1.call-update) | async-done | bytes 98320 | tf_op jit(solution)/shard_map/psum | solution.py:92
  174.1 0.9 fusion.25
  175.0 0.1 multiply_reduce_fusion
  175.2 4.6 %convolution_multiply_fusion.1 = f32[8,1056]{1,0:T(8,128)S(1)} fusion(bf16[3072,1056]{0,1:T(8,128)(2,1)} %param.31, f32[3072]{0:T(1024)S(1)} %copy-done.7, bf16[8,3072]{1,0:T(8,128)(2,1)S(1)} %fusion.25, f32[8]{0:T(128)S(1)} %add_rsqrt_fusion), kind=kOutput, calls=%fused_computation.2 | convolution fusion | flops 51986688 | bytes 6583328 | tf_op jit(solution)/shard_map/dot_general | solution.py:97
  179.8 4.6 %fusion.2 = bf16[1,1056,8]{1,2,0:T(8,128)(2,1)S(1)} fusion(bf16[3072,1056]{0,1:T(8,128)(2,1)} %param.32, f32[3072]{0:T(1024)S(1)} %copy-done.7, bf16[8,3072]{1,0:T(8,128)(2,1)S(1)} %fusion.25, f32[8,1056]{1,0:T(8,128)S(1)} %convolution_multiply_fusion.1, f32[8]{0:T(128)S(1)} %add_rsqrt_fusion), kind=kOutput, calls=%fused_computation.4 | convolution fusion | flops 52037376 | bytes 6600224 | tf_op jit(solution)/shard_map/dot_general | solution.py:98
  184.4 30.7 %all-gather = bf16[8,1056,8]{1,2,0:T(8,128)(2,1)S(1)} all-gather(bf16[1,1056,8]{1,2,0:T(8,128)(2,1)S(1)} %fusion.2), channel_id=1, replica_groups=mesh['dp'=2,'kv'=8,'tp'=2] {'kv'}, dimensions={0}, use_global_device_ids=true | all-gather | bytes 152064 | tf_op jit(solution)/shard_map/all_gather | solution.py:102
  215.1 0.1 reshape.385
  215.3 4.4 %fusion.11 = bf16[8,384]{1,0:T(8,128)(2,1)} fusion(bf16[8448,8]{0,1:T(8,128)(2,1)S(1)} %reshape.385, bf16[8448,384]{1,0:T(8,128)(2,1)} %param.33, f32[8,3072]{1,0:T(8,128)S(1)} %convert_element_type.150, s32[]{:T(128)S(6)} %select_n.14), kind=kOutput, calls=%fused_computation.19 | convolution fusion | flops 51910656 | bytes 6641668 | tf_op jit(solution)/shard_map/dot_general | solution.py:101
  (41 shorter events, 0.6 us)
Async XLA Ops:
  7.2 98.2 %copy-start = (bf16[384,3072]{1,0:T(8,128)(2,1)S(1)}, bf16[384,3072]{1,0:T(8,128)(2,1)}, u32[]{:S(2)}) copy-start(bf16[384,3072]{1,0:T(8,128)(2,1)} %param.29) | copy-start | bytes 7077892
  44.9 14.9 %all-to-all-start = ((bf16[8,2,192]{2,1,0:T(2,128)(2,1)}), bf16[8,2,192]{2,1,0:T(2,128)(2,1)S(1)}, u32[]{:S(2)}, u32[]{:S(2)}) async-start(bf16[8,2,192]{2,1,0:T(2,128)(2,1)} %reshape.400), calls=%async_computation | async-start | bytes 16384 | tf_op jit(solution)/shard_map/all_to_all | solution.py:60
  50.3 2.8 %copy-start.3 = (bf16[3072,384]{1,0:T(8,128)(2,1)S(1)}, bf16[3072,384]{1,0:T(8,128)(2,1)}, u32[]{:S(2)}) copy-start(bf16[3072,384]{1,0:T(8,128)(2,1)} %param.20) | copy-start | bytes 7077892
  50.9 2.7 %copy-start.4 = (bf16[3072,384]{1,0:T(8,128)(2,1)S(1)}, bf16[3072,384]{1,0:T(8,128)(2,1)}, u32[]{:S(2)}) copy-start(bf16[3072,384]{1,0:T(8,128)(2,1)} %param.23) | copy-start | bytes 7077892
  53.1 1.0 copy-start.5
  53.1 1.0 copy-start.8
  53.1 1.0 copy-start.9
  53.1 1.8 copy-start.6
  59.8 12.5 %all-to-all-start.1 = ((bf16[8,2,192]{2,1,0:T(2,128)(2,1)}), bf16[8,2,192]{2,1,0:T(2,128)(2,1)S(1)}, u32[]{:S(2)}, u32[]{:S(2)}) async-start(bf16[8,2,192]{2,1,0:T(2,128)(2,1)} %reshape.402), calls=%async_computation.1 | async-start | bytes 16384 | tf_op jit(solution)/shard_map/all_to_all | solution.py:61
  72.3 9.8 %all-to-all-start.2 = ((bf16[8,2,192]{2,1,0:T(2,128)(2,1)}), bf16[8,2,192]{2,1,0:T(2,128)(2,1)S(1)}, u32[]{:S(2)}, u32[]{:S(2)}) async-start(bf16[8,2,192]{2,1,0:T(2,128)(2,1)} %reshape.398), calls=%async_computation.2 | async-start | bytes 16384 | tf_op jit(solution)/shard_map/all_to_all | solution.py:59
  82.1 10.0 %all-to-all-start.3 = ((bf16[8,2,192]{2,1,0:T(2,128)(2,1)}), bf16[8,2,192]{2,1,0:T(2,128)(2,1)S(1)}, u32[]{:S(2)}, u32[]{:S(2)}) async-start(bf16[8,2,192]{2,1,0:T(2,128)(2,1)} %reshape.396), calls=%async_computation.3 | async-start | bytes 16384 | tf_op jit(solution)/shard_map/all_to_all | solution.py:62
  85.4 88.6 %all-reduce.2.cloned.1.call-start = ((), (), s32[]{:S(2)}) async-start(), calls=%async_computation.5 | async-start | bytes 196608 | tf_op jit(solution)/shard_map/psum | solution.py:92
  85.6 3.2 %copy-start.1 = (f32[1,24,128,128]{3,2,1,0:T(8,128)S(1)}, f32[1,24,128,128]{3,2,1,0:T(8,128)}, u32[]{:S(2)}) copy-start(f32[1,24,128,128]{3,2,1,0:T(8,128)} %param.18) | copy-start | bytes 4718596
  88.8 3.4 %copy-start.10 = (f32[128]{0:T(128)S(1)}, f32[128]{0:T(128)}, u32[]{:S(2)}) copy-start(f32[128]{0:T(128)} %param.28) | copy-start | bytes 1540
  89.4 1.1 copy-start.2
  90.5 84.6 %copy-start.7 = (f32[3072]{0:T(1024)S(1)}, f32[3072]{0:T(1024)}, u32[]{:S(2)}) copy-start(f32[3072]{0:T(1024)} %param.30) | copy-start | bytes 36868
Sparse Core Ops, SparseCore 0:
  106.6 67.4 all-reduce.1
where the time goes:
time: 227 us
  waiting for transfers between devices  80.3 us (35%)
  blocking collectives  75.8 us (33%)
  matrix products  25.8 us (11%)
  starting transfers between devices  18.1 us (8%)
  between operations  14.3 us (6%)
  other arithmetic  6.49 us (3%)
  local copies, waits for them, and re-layouts  5.82 us (3%)
    psum x1, waiting for transfers between devices, body(): mixer_out = lax.psum(partial_out, 'kv')  67.6 us
    all_gather x1, blocking collectives, body(): complete_rows = lax.all_gather(tokens, 'kv', axis=1, tiled=True)  32.9 us
    all_gather x1, blocking collectives, body(): lax.all_gather(hidden_units, 'kv', axis=1, tiled=True)  30.7 us
    all_to_all x1, blocking collectives, body(): lax.all_to_all(gated_read, 'kv', split_axis=1, concat_axis=0, tiled=True)  12.2 us
    all_to_all x1, waiting for transfers between devices, body(): lax.all_to_all(query_cols, 'kv', split_axis=0, concat_axis=1, tiled=True)  6.33 us
    all_to_all x1, waiting for transfers between devices, body(): lax.all_to_all(value_cols, 'kv', split_axis=0, concat_axis=1, tiled=True)  6.29 us
    all_to_all x1, starting transfers between devices, body(): lax.all_to_all(value_cols, 'kv', split_axis=0, concat_axis=1, tiled=True)  5.99 us
    all_to_all x1, starting transfers between devices, body(): lax.all_to_all(key_cols, 'kv', split_axis=0, concat_axis=1, tiled=True)  5.36 us
  transfers between devices with their start and end apart: 5, of which 3 were waited for; matrix products, arithmetic and copies ran while one was open for 7% of the time, Pallas kernels for 0%

commit v1 on v0

v1 whole, which is shorter than its diff:
```python
import jax
import jax.numpy as jnp
from jax import lax
from jax.sharding import PartitionSpec as P

HEAD_DIM = 128
EPS = 1e-06


def norm_scale(values):
    return lax.rsqrt(jnp.mean(values * values, axis=-1, keepdims=True) + EPS)


def unit_rows(values):
    return values * lax.rsqrt(jnp.sum(values * values, axis=-1, keepdims=True) + EPS)


def gather_kv(block, parts):
    copies = jnp.broadcast_to(block[None], (parts,) + block.shape)
    return lax.all_to_all(copies, "kv", split_axis=0, concat_axis=0, tiled=True)


def body(
    tokens,
    old_state,
    mixer_gain,
    w_query,
    w_key,
    w_value,
    w_outgate,
    w_decay,
    w_write,
    decay_log,
    decay_bias,
    head_gain,
    w_output,
    channel_gain,
    w_gate,
    w_up,
    w_down,
    *,
    parts,
):
    f32, bf16 = jnp.float32, jnp.bfloat16
    rows, share = tokens.shape
    width = share * parts
    local_rows, heads = old_state.shape[:2]
    head_cols = w_query.shape[1]
    place = lax.axis_index("kv")

    tok_wide = gather_kv(tokens, parts).transpose(1, 0, 2).reshape(rows, width).astype(f32)
    scale_in = norm_scale(tok_wide)
    normed = (tok_wide * mixer_gain).astype(bf16)

    def project(weight):
        return (jnp.dot(normed, weight, preferred_element_type=f32) * scale_in).astype(bf16)

    packed = jnp.stack([project(w) for w in (w_query, w_key, w_value, w_outgate)], axis=1)
    packed = packed.reshape(parts, local_rows, 4, head_cols)
    packed = lax.all_to_all(packed, "kv", split_axis=0, concat_axis=0, tiled=True)

    own_normed = lax.dynamic_slice_in_dim(normed, place * local_rows, local_rows, 0)
    own_scale = lax.dynamic_slice_in_dim(scale_in, place * local_rows, local_rows, 0)
    decay_pre = jnp.dot(own_normed, w_decay, preferred_element_type=f32) * own_scale
    write_pre = jnp.dot(own_normed, w_write, preferred_element_type=f32) * own_scale

    def by_head(index):
        chosen = packed[:, :, index].transpose(1, 0, 2)
        return chosen.reshape(local_rows, heads, HEAD_DIM).astype(f32)

    queries = unit_rows(jax.nn.silu(by_head(0))) * HEAD_DIM ** (-0.5)
    keys_unit = unit_rows(jax.nn.silu(by_head(1)))
    values_act = jax.nn.silu(by_head(2))
    strength = jax.nn.sigmoid(write_pre)
    retain = jnp.exp(-jnp.exp(decay_log) * jax.nn.softplus(decay_pre + decay_bias))
    recalled = jnp.einsum("bhkv,bhk->bhv", old_state, keys_unit, precision=lax.Precision.HIGHEST)
    correction = values_act - retain[..., None] * recalled
    new_state = (
        retain[..., None, None] * old_state
        + (strength[..., None] * keys_unit)[..., :, None] * correction[..., None, :]
    )
    readout = jnp.einsum("bhkv,bhk->bhv", new_state, queries, precision=lax.Precision.HIGHEST)
    gated_read = readout * norm_scale(readout) * head_gain * jax.nn.silu(by_head(3))
    gated_read = gated_read.reshape(local_rows, parts, head_cols).astype(bf16).transpose(1, 0, 2)
    read_cols = lax.all_to_all(gated_read, "kv", split_axis=0, concat_axis=0, tiled=True)
    read_cols = read_cols.reshape(rows, head_cols)

    partial_out = jnp.dot(read_cols, w_output, preferred_element_type=f32)
    partial_out = partial_out.reshape(rows, parts, share).transpose(1, 0, 2)
    mixer_out = lax.all_to_all(partial_out, "kv", split_axis=0, concat_axis=0, tiled=True).sum(0)
    own_residual = (tokens.astype(f32) + mixer_out).astype(bf16)
    residual = gather_kv(own_residual, parts).transpose(1, 0, 2).reshape(rows, width)
    residual_wide = residual.astype(f32)
    scale_mid = norm_scale(residual_wide)
    normed_mid = (residual_wide * channel_gain).astype(bf16)
    gate_act = jnp.dot(normed_mid, w_gate, preferred_element_type=f32) * scale_mid
    upward = jnp.dot(normed_mid, w_up, preferred_element_type=f32) * scale_mid
    hidden = (jax.nn.silu(gate_act) * upward).astype(bf16)
    hidden = gather_kv(hidden, parts).transpose(1, 0, 2).reshape(rows, -1)
    down_sum = jnp.dot(hidden, w_down, preferred_element_type=f32)
    mixed = (own_residual.astype(f32) + down_sum).astype(bf16)
    return (mixed, new_state)


def solution(mesh):
    parts = mesh.shape["kv"]
    rows, states = P(("tp", "dp"), "kv"), P(("tp", "dp", "kv"), None, None, None)
    cols = P(None, "kv")
    in_specs = (rows, states, P(), cols, cols, cols, cols, P(), P(), P(), P(), P())
    in_specs += (P("kv", None), P(), cols, cols, cols)

    def step(*args):
        return body(*args, parts=parts)

    return jax.shard_map(
        step, mesh=mesh, in_specs=in_specs, out_specs=(rows, states), check_vma=False
    )
```

time: 227 us -> 96.6 us (0.43)
  waiting for transfers between devices: 80.3 us -> 13.9 us
  blocking collectives: 75.8 us -> 29.7 us
  between operations: 14.3 us -> 0.89 us
  local copies, waits for them, and re-layouts: 5.82 us -> 10.9 us
  starting transfers between devices: 18.1 us -> 14 us
  other arithmetic: 6.49 us -> 3.04 us
  matrix products: 25.8 us -> 23.5 us
    psum x1 -> x0, waiting for transfers between devices: 67.6 us -> none  [body(): mixer_out = lax.psum(partial_out, 'kv')]
    all_gather x2 -> x0, blocking collectives: 63.6 us -> none  [the longest x1 32.9 us: body(): complete_rows = lax.all_gather(tokens, 'kv', axis=1, tiled=True)]
    all_to_all x1 -> x3, blocking collectives: 12.2 us -> 29.7 us  [the longest x2 19 us: gather_kv(): return lax.all_to_all(copies, 'kv', split_axis=0, concat_axis=0, tiled=True)]
    dot_general x0 -> x1, local copies, waits for them, and re-layouts: none -> 4.3 us  [body(): partial_out = jnp.dot(read_cols, w_output, preferred_element_type=f32)]
    all_to_all x4 -> x3, starting transfers between devices: 18 us -> 14 us  [the longest x1 7.31 us: gather_kv(): return lax.all_to_all(copies, 'kv', split_axis=0, concat_axis=0, tiled=True)]
    all_to_all x4 -> x0, other arithmetic: 2.61 us -> none  [the longest x1 0.67 us: body(): lax.all_to_all(value_cols, 'kv', split_axis=0, concat_axis=1, tiled=True)]
    unnamed x33 -> x28, local copies, waits for them, and re-layouts: 4.66 us -> 3.18 us
    all_to_all x4 -> x3, waiting for transfers between devices: 12.6 us -> 13.9 us  [the longest x1 6.8 us: gather_kv(): return lax.all_to_all(copies, 'kv', split_axis=0, concat_axis=0, tiled=True)]
  transfers between devices with their start and end apart: 5 -> 3, of which waited for: 3 -> 3; matrix products, arithmetic and copies ran while one was open for 7% -> 6% of each run, Pallas kernels for 0% -> 0%
where the time goes in v1:
time: 96.6 us; the launch traced here: 95.9 us
  blocking collectives  29.7 us (31%)
  matrix products  23.5 us (24%)
  starting transfers between devices  14 us (14%)
  waiting for transfers between devices  13.9 us (14%)
  local copies, waits for them, and re-layouts  10.9 us (11%)
  other arithmetic  3.04 us (3%)
    all_to_all x2, blocking collectives, gather_kv(): return lax.all_to_all(copies, 'kv', split_axis=0, concat_axis=0, tiled=True)  19 us
    all_to_all x1, blocking collectives, body(): lax.all_to_all(partial_out, 'kv', split_axis=0, concat_axis=0, tiled=True)  10.7 us
    all_to_all x1, starting transfers between devices, gather_kv(): return lax.all_to_all(copies, 'kv', split_axis=0, concat_axis=0, tiled=True)  7.31 us
    all_to_all x1, waiting for transfers between devices, gather_kv(): return lax.all_to_all(copies, 'kv', split_axis=0, concat_axis=0, tiled=True)  6.8 us
    all_to_all x1, waiting for transfers between devices, body(): lax.all_to_all(packed, 'kv', split_axis=0, concat_axis=0, tiled=True)  4.9 us
    dot_general x1, matrix products, body(): upward = jnp.dot(normed_mid, w_up, preferred_element_type=f32) * scale_mid  4.64 us
    dot_general x1, matrix products, body(): jnp.dot(normed_mid, w_gate, preferred_element_type=f32) * scale_mid  4.62 us
    dot_general x1, matrix products, body(): down_sum = jnp.dot(hidden, w_down, preferred_element_type=f32)  4.4 us
  transfers between devices with their start and end apart: 3, of which 3 were waited for; matrix products, arithmetic and copies ran while one was open for 6% of the time, Pallas kernels for 0%

profile of v1, /device:TPU:0, one launch (start us, length us, event | category | flops | bytes accessed | tf_op | source)
XLA Modules:
  0.0 95.9 jit_solution(1096887852980575542)
XLA Ops:
  0.6 0.0 copy-start
  0.6 1.5 %broadcast_in_dim.6 = bf16[8,8,384]{2,1,0:T(8,128)(2,1)} broadcast(bf16[8,384]{1,0:T(8,128)(2,1)} %param.17), dimensions={1,2} | broadcast | bytes 55296 | tf_op jit(solution)/shard_map/broadcast_in_dim | solution.py:19
  2.1 7.3 %all-to-all-start = ((bf16[8,8,384]{2,1,0:T(8,128)(2,1)}), bf16[8,8,384]{2,1,0:T(8,128)(2,1)S(1)}, u32[]{:S(2)}, u32[]{:S(2)}) async-start(bf16[8,8,384]{2,1,0:T(8,128)(2,1)} %broadcast_in_dim.6), calls=%async_computation | async-start | bytes 98304 | tf_op jit(solution)/shard_map/all_to_all | solution.py:20
  9.4 6.8 %all-to-all-done = bf16[8,8,384]{2,1,0:T(8,128)(2,1)S(1)} async-done(((bf16[8,8,384]{2,1,0:T(8,128)(2,1)}), bf16[8,8,384]{2,1,0:T(8,128)(2,1)S(1)}, u32[]{:S(2)}, u32[]{:S(2)}) %all-to-all-start) | async-done | bytes 49184 | tf_op jit(solution)/shard_map/all_to_all | solution.py:20
  16.2 0.1 multiply_reduce_fusion.1
  16.4 0.6 dynamic-slice.3
  17.0 0.7 multiply_convert_fusion.1
  17.7 0.0 copy-start.4
  17.7 0.4 fusion.11
  18.1 0.0 copy-done.3
  18.1 0.0 copy-start.5
  18.2 0.4 fusion.12
  18.6 0.9 copy-done.4
  19.4 0.4 fusion.13
  19.8 0.4 copy-done.5
  20.2 0.4 fusion.14
  20.6 0.6 copy.28
  21.2 3.3 %all-to-all-start.1 = ((bf16[8,1,4,384]{3,2,1,0:T(4,128)(2,1)}), bf16[8,1,4,384]{3,2,1,0:T(4,128)(2,1)S(1)}, u32[]{:S(2)}, u32[]{:S(2)}) async-start(bf16[8,1,4,384]{3,2,1,0:T(4,128)(2,1)} %copy.28), calls=%async_computation.1 | async-start | bytes 49152 | tf_op jit(solution)/shard_map/all_to_all | solution.py:60
  24.6 0.8 fusion.31
  25.4 0.8 fusion.19
  26.3 4.9 %all-to-all-done.1 = bf16[8,1,4,384]{3,2,1,0:T(4,128)(2,1)S(1)} async-done(((bf16[8,1,4,384]{3,2,1,0:T(4,128)(2,1)}), bf16[8,1,4,384]{3,2,1,0:T(4,128)(2,1)S(1)}, u32[]{:S(2)}, u32[]{:S(2)}) %all-to-all-start.1) | async-done | bytes 24608 | tf_op jit(solution)/shard_map/all_to_all | solution.py:60
  31.2 0.1 multiply_reduce_fusion.4
  31.3 0.1 multiply_reduce_fusion.3
  31.5 0.1 multiply_multiply_fusion
  31.5 0.1 broadcast_multiply_fusion
  31.6 2.8 %fusion.4 = f32[24,1,128]{2,1,0:T(1,128)S(1)} fusion(f32[24,128,1]{1,2,0:T(1,128)S(1)} %bitcast.108, f32[1,24,128,128]{3,2,1,0:T(8,128)} %param.18), kind=kOutput, calls=%fused_computation.6 | convolution fusion | flops 4718592 | bytes 1597440 | tf_op jit(solution)/shard_map/bhkv,bhk->bhv/dot_general | solution.py:76
  34.4 0.1 multiply_subtract_fusion
  34.5 0.6 multiply_add_fusion
  35.1 1.1 %copy-done.2 = f32[1,24,128,128]{3,2,1,0:T(8,128)} copy-done((f32[1,24,128,128]{3,2,1,0:T(8,128)}, f32[1,24,128,128]{3,2,1,0:T(8,128)S(1)}, u32[]{:S(2)}) %copy-start.2) | copy-done | bytes 1572888
  36.2 1.4 %fusion.2 = f32[24,1,128]{2,1,0:T(1,128)S(1)} fusion(f32[24,128,1]{1,2,0:T(1,128)S(1)} %bitcast.107, f32[1,24,128,128]{3,2,1,0:T(8,128)S(1)} %multiply_add_fusion), kind=kOutput, calls=%fused_computation.4 | convolution fusion | flops 4718592 | bytes 1597440 | tf_op jit(solution)/shard_map/bhkv,bhk->bhv/dot_general | solution.py:82
  37.7 0.1 multiply_reduce_fusion.2
  37.8 0.1 multiply_convert_fusion.4
  37.9 0.5 broadcast.218
  38.4 0.7 reduce.8
  39.1 0.7 reshape.359
  39.8 3.3 %all-to-all-start.2 = ((bf16[8,2,192]{2,1,0:T(2,128)(2,1)}), bf16[8,2,192]{2,1,0:T(2,128)(2,1)S(1)}, u32[]{:S(2)}, u32[]{:S(2)}) async-start(bf16[8,2,192]{2,1,0:T(2,128)(2,1)} %reshape.359), calls=%async_computation.2 | async-start | bytes 16384 | tf_op jit(solution)/shard_map/all_to_all | solution.py:85
  43.1 4.3 %copy.36 = bf16[3072,384]{1,0:T(8,128)(2,1)} copy(bf16[3072,384]{0,1:T(8,128)(2,1)} %bitcast.96) | data formatting | bytes 4718592 | tf_op jit(solution)/shard_map/dot_general | solution.py:88
  47.4 2.2 %all-to-all-done.2 = bf16[8,2,192]{2,1,0:T(2,128)(2,1)S(1)} async-done(((bf16[8,2,192]{2,1,0:T(2,128)(2,1)}), bf16[8,2,192]{2,1,0:T(2,128)(2,1)S(1)}, u32[]{:S(2)}, u32[]{:S(2)}) %all-to-all-start.2) | async-done | bytes 6176 | tf_op jit(solution)/shard_map/all_to_all | solution.py:85
  49.6 0.1 reshape.360
  49.7 2.4 %convolution_bitcast_fusion = f32[8,8,384]{2,1,0:T(8,128)S(1)} fusion(bf16[8,384,384]{2,1,0:T(8,128)(2,1)} %bitcast.95, bf16[8,1,384]{2,1,0:T(2,128)(2,1)S(1)} %reshape.360), kind=kOutput, calls=%fused_computation.9 | convolution fusion | flops 18874368 | bytes 2463744 | tf_op jit(solution)/shard_map/dot_general | solution.py:88
  52.0 10.7 %all_to_all.30 = f32[8,8,384]{2,1,0:T(8,128)S(1)} all-to-all(f32[8,8,384]{2,1,0:T(8,128)S(1)} %convolution_bitcast_fusion), channel_id=1, replica_groups=mesh['dp'=2,'kv'=8,'tp'=2] {'kv'}, dimensions={0} | all-to-all | bytes 196608 | tf_op jit(solution)/shard_map/all_to_all | solution.py:90
  62.8 9.2 %all_to_all.31 = bf16[8,8,384]{2,1,0:T(8,128)(2,1)S(1)} all-to-all(bf16[8,8,384]{2,1,0:T(8,128)(2,1)S(1)} %broadcast_in_dim.7), channel_id=1, replica_groups=mesh['dp'=2,'kv'=8,'tp'=2] {'kv'}, dimensions={0} | all-to-all | bytes 98304 | tf_op jit(solution)/shard_map/all_to_all | solution.py:20
  72.0 0.1 multiply_reduce_fusion
  72.1 4.6 %convolution_multiply_fusion.1 = f32[8,1056]{1,0:T(8,128)S(1)} fusion(bf16[3072,1056]{0,1:T(8,128)(2,1)} %param.31, f32[8]{0:T(128)S(1)} %add_rsqrt_fusion, f32[8,3072]{1,0:T(8,128)S(1)} %bitcast.97, f32[3072]{0:T(1024)S(1)} %copy-done.8), kind=kOutput, calls=%fused_computation.2 | convolution fusion | flops 51962112 | bytes 6632480 | tf_op jit(solution)/shard_map/dot_general | solution.py:96
  76.8 4.6 %fusion.1 = bf16[8,1056]{1,0:T(8,128)(2,1)S(1)} fusion(bf16[3072,1056]{0,1:T(8,128)(2,1)} %param.32, f32[8,1056]{1,0:T(8,128)S(1)} %convolution_multiply_fusion.1, f32[8]{0:T(128)S(1)} %add_rsqrt_fusion, f32[8,3072]{1,0:T(8,128)S(1)} %bitcast.98, f32[3072]{0:T(1024)S(1)} %copy-done.8), kind=kOutput, calls=%fused_computation.3 | convolution fusion | flops 52012800 | bytes 6649376 | tf_op jit(solution)/shard_map/dot_general | solution.py:97
  81.5 9.8 %all_to_all.32 = bf16[8,8,1056]{2,1,0:T(8,128)(2,1)S(1)} all-to-all(bf16[8,8,1056]{2,1,0:T(8,128)(2,1)S(1)} %broadcast_in_dim.8), channel_id=1, replica_groups=mesh['dp'=2,'kv'=8,'tp'=2] {'kv'}, dimensions={0} | all-to-all | bytes 270336 | tf_op jit(solution)/shard_map/all_to_all | solution.py:20
  91.3 0.1 reshape.338
  91.5 4.4 %fusion.10 = bf16[8,384]{1,0:T(8,128)(2,1)} fusion(bf16[8,8448]{1,0:T(8,128)(2,1)S(1)} %reshape.338, bf16[8448,384]{1,0:T(8,128)(2,1)} %param.33, bf16[8,384]{1,0:T(8,128)(2,1)S(1)} %add_convert_fusion), kind=kOutput, calls=%fused_computation.19 | convolution fusion | flops 51913728 | bytes 6635520 | tf_op jit(solution)/shard_map/dot_general | solution.py:100
  (34 shorter events, 0.2 us)
Async XLA Ops:
  0.6 17.1 %copy-start = (bf16[3072,384]{1,0:T(8,128)(2,1)S(1)}, bf16[3072,384]{1,0:T(8,128)(2,1)}, u32[]{:S(2)}) copy-start(bf16[3072,384]{1,0:T(8,128)(2,1)} %param.23) | copy-start | bytes 7077892
  2.1 14.1 %all-to-all-start = ((bf16[8,8,384]{2,1,0:T(8,128)(2,1)}), bf16[8,8,384]{2,1,0:T(8,128)(2,1)S(1)}, u32[]{:S(2)}, u32[]{:S(2)}) async-start(bf16[8,8,384]{2,1,0:T(8,128)(2,1)} %broadcast_in_dim.6), calls=%async_computation | async-start | bytes 98304 | tf_op jit(solution)/shard_map/all_to_all | solution.py:20
  16.2 1.9 %copy-start.3 = (bf16[3072,384]{1,0:T(8,128)(2,1)S(1)}, bf16[3072,384]{1,0:T(8,128)(2,1)}, u32[]{:S(2)}) copy-start(bf16[3072,384]{1,0:T(8,128)(2,1)} %param.22) | copy-start | bytes 7077892
  17.7 1.7 %copy-start.4 = (bf16[3072,384]{1,0:T(8,128)(2,1)S(1)}, bf16[3072,384]{1,0:T(8,128)(2,1)}, u32[]{:S(2)}) copy-start(bf16[3072,384]{1,0:T(8,128)(2,1)} %param.21) | copy-start | bytes 7077892
  18.1 2.0 %copy-start.5 = (bf16[3072,384]{1,0:T(8,128)(2,1)S(1)}, bf16[3072,384]{1,0:T(8,128)(2,1)}, u32[]{:S(2)}) copy-start(bf16[3072,384]{1,0:T(8,128)(2,1)} %param.20) | copy-start | bytes 7077892
  19.4 5.2 %copy-start.6 = (bf16[3072,24]{0,1:T(8,128)(2,1)S(1)}, bf16[3072,24]{0,1:T(8,128)(2,1)}, u32[]{:S(2)}) copy-start(bf16[3072,24]{0,1:T(8,128)(2,1)} %param.24) | copy-start | bytes 442372
  19.4 5.2 %copy-start.10 = (f32[24]{0:T(128)S(1)}, f32[24]{0:T(128)}, u32[]{:S(2)}) copy-start(f32[24]{0:T(128)} %param.27) | copy-start | bytes 292
  19.4 5.2 %copy-start.11 = (f32[24]{0:T(128)S(1)}, f32[24]{0:T(128)}, u32[]{:S(2)}) copy-start(f32[24]{0:T(128)} %param.26) | copy-start | bytes 292
  19.4 6.0 %copy-start.7 = (bf16[3072,24]{0,1:T(8,128)(2,1)S(1)}, bf16[3072,24]{0,1:T(8,128)(2,1)}, u32[]{:S(2)}) copy-start(bf16[3072,24]{0,1:T(8,128)(2,1)} %param.25) | copy-start | bytes 442372
  21.2 9.9 %all-to-all-start.1 = ((bf16[8,1,4,384]{3,2,1,0:T(4,128)(2,1)}), bf16[8,1,4,384]{3,2,1,0:T(4,128)(2,1)S(1)}, u32[]{:S(2)}, u32[]{:S(2)}) async-start(bf16[8,1,4,384]{3,2,1,0:T(4,128)(2,1)} %copy.28), calls=%async_computation.1 | async-start | bytes 49152 | tf_op jit(solution)/shard_map/all_to_all | solution.py:60
  31.2 3.4 %copy-start.1 = (f32[1,24,128,128]{3,2,1,0:T(8,128)S(1)}, f32[1,24,128,128]{3,2,1,0:T(8,128)}, u32[]{:S(2)}) copy-start(f32[1,24,128,128]{3,2,1,0:T(8,128)} %param.18) | copy-start | bytes 4718596
  34.5 3.3 %copy-start.12 = (f32[128]{0:T(128)S(1)}, f32[128]{0:T(128)}, u32[]{:S(2)}) copy-start(f32[128]{0:T(128)} %param.28) | copy-start | bytes 1540
  35.1 1.1 %copy-start.2 = (f32[1,24,128,128]{3,2,1,0:T(8,128)}, f32[1,24,128,128]{3,2,1,0:T(8,128)S(1)}, u32[]{:S(2)}) copy-start(f32[1,24,128,128]{3,2,1,0:T(8,128)S(1)} %multiply_add_fusion) | copy-start | bytes 4718596
  39.8 9.8 %all-to-all-start.2 = ((bf16[8,2,192]{2,1,0:T(2,128)(2,1)}), bf16[8,2,192]{2,1,0:T(2,128)(2,1)S(1)}, u32[]{:S(2)}, u32[]{:S(2)}) async-start(bf16[8,2,192]{2,1,0:T(2,128)(2,1)} %reshape.359), calls=%async_computation.2 | async-start | bytes 16384 | tf_op jit(solution)/shard_map/all_to_all | solution.py:85
  47.4 15.3 %copy-start.9 = (bf16[8,384]{1,0:T(8,128)(2,1)S(1)}, bf16[8,384]{1,0:T(8,128)(2,1)}, u32[]{:S(2)}) copy-start(bf16[8,384]{1,0:T(8,128)(2,1)} %param.17) | copy-start | bytes 18436
  47.4 24.7 %copy-start.8 = (f32[3072]{0:T(1024)S(1)}, f32[3072]{0:T(1024)}, u32[]{:S(2)}) copy-start(f32[3072]{0:T(1024)} %param.30) | copy-start | bytes 36868

commit v2 on v1

v2 whole, which is shorter than its diff:
```python
import functools

import jax
import jax.numpy as jnp
from jax import lax
from jax.experimental import pallas as pl
from jax.experimental.pallas import tpu as pltpu
from jax.sharding import PartitionSpec as P

HEAD_DIM = 128
EPS = 1e-06
MIB = 1 << 20
SLOTS = 16

F32, BF16 = jnp.float32, jnp.bfloat16


def norm_scale(values):
    return lax.rsqrt(jnp.mean(values * values, axis=-1, keepdims=True) + EPS)


def unit_rows(values):
    return values * lax.rsqrt(jnp.sum(values * values, axis=-1, keepdims=True) + EPS)


def silu(values):
    return values / (1.0 + jnp.exp(-values))


def exchange(slabs):
    return lax.all_to_all(slabs, "kv", split_axis=0, concat_axis=0, tiled=True)


def gather_kv(block, parts):
    return exchange(jnp.broadcast_to(block[None], (parts,) + block.shape))


def call(kernel, out_shape, args, *, limit=8, scratch=(), spaces=None, span=8):
    vmem = pl.BlockSpec(memory_space=pltpu.VMEM)
    specs = [vmem] * len(args) if spaces is None else spaces
    many = isinstance(out_shape, (tuple, list))
    return pl.pallas_call(
        kernel,
        out_shape=out_shape,
        in_specs=specs,
        out_specs=[vmem] * len(out_shape) if many else vmem,
        scratch_shapes=list(scratch),
        compiler_params=pltpu.CompilerParams(vmem_limit_bytes=limit * MIB),
        cost_estimate=pl.CostEstimate(
            flops=span * 500_000_000, bytes_accessed=span * 3_000_000, transcendentals=0
        ),
    )(*args)


def wide_rows(ref, parts):
    return jnp.concatenate([ref[s] for s in range(parts)], axis=-1)


def eye(n):
    across = lax.broadcasted_iota(jnp.int32, (n, n), 1)
    return lax.broadcasted_iota(jnp.int32, (n, n), 0) == across


def upright(row):
    return jnp.sum(jnp.where(eye(row.shape[1]), row, 0.0), axis=1, keepdims=True)


def spread_kernel(block_ref, out_ref, *, parts):
    for s in range(parts):
        out_ref[s] = block_ref[...]


def project_kernel(
    x_ref, gain_ref, wq, wk, wv, wg, wd_ref, ww_ref, log_ref, bias_ref,
    slab_ref, retain_ref, strength_ref, scr, *, parts, tiles,
):
    x = wide_rows(x_ref, parts).astype(F32)
    scale = norm_scale(x)
    normed = (x * gain_ref[...]).astype(BF16)
    scr[:, 4 * tiles :, :] = jnp.zeros((x.shape[0], SLOTS - 4 * tiles, HEAD_DIM), F32)
    for i, w in enumerate((wq, wk, wv, wg)):
        acc = jnp.dot(normed, w[...], preferred_element_type=F32) * scale
        for t in range(tiles):
            scr[:, i * tiles + t, :] = acc[:, t * HEAD_DIM : (t + 1) * HEAD_DIM]
    slab_ref[...] = scr[...].astype(BF16)
    lane_scale = jnp.sum(jnp.where(eye(x.shape[0]), scale, 0.0), axis=0, keepdims=True)
    nt = (((1,), (1,)), ((), ()))
    decay = lax.dot_general(wd_ref[...], normed, nt, preferred_element_type=F32) * lane_scale
    write = lax.dot_general(ww_ref[...], normed, nt, preferred_element_type=F32) * lane_scale
    pre = decay + upright(bias_ref[...])
    soft = jnp.maximum(pre, 0.0) + jnp.log1p(jnp.exp(-jnp.abs(pre)))
    retain_ref[...] = jnp.exp(-jnp.exp(upright(log_ref[...])) * soft)
    strength_ref[...] = 1.0 / (1.0 + jnp.exp(-write))


def state_kernel(
    place_ref, slab_ref, s_ref, retain_ref, strength_ref, gain_ref,
    read_ref, new_ref, ro, *, parts, tiles,
):
    place = place_ref[0]
    act = silu(slab_ref[...].astype(F32))
    total = jnp.sum(act * act, axis=-1, keepdims=True)
    slot = lax.broadcasted_iota(jnp.int32, act.shape[:2] + (1,), 1)
    factor = lax.rsqrt(total + EPS)
    factor = jnp.where(slot < tiles, factor * HEAD_DIM ** (-0.5), factor)
    factor = jnp.where(slot < 2 * tiles, factor, 1.0)
    unit = act * factor
    ro[...] = jnp.zeros(ro.shape, F32)
    columns = unit.reshape(parts * SLOTS, HEAD_DIM).T
    lane = lax.broadcasted_iota(jnp.int32, retain_ref.shape, 1)
    own = lane == place
    retain = jnp.sum(jnp.where(own, retain_ref[...], 0.0), axis=1, keepdims=True)
    strength = jnp.sum(jnp.where(own, strength_ref[...], 0.0), axis=1, keepdims=True)
    heads = parts * tiles
    retain = jnp.broadcast_to(retain, (heads, HEAD_DIM))
    strength = jnp.broadcast_to(strength, (heads, HEAD_DIM))
    for h in range(heads):
        j, t = divmod(h, tiles)
        base = j * SLOTS + t
        query = columns[:, base : base + 1]
        key = columns[:, base + tiles : base + tiles + 1]
        value = unit[j, 2 * tiles + t : 2 * tiles + t + 1, :]
        old = s_ref[h]
        keep = retain[h : h + 1, :]
        recalled = jnp.sum(old * key, axis=0, keepdims=True)
        correction = (value - keep * recalled) * strength[h : h + 1, :]
        new = keep * old + key * correction
        new_ref[h] = new
        ro[j, 3 * tiles + t : 3 * tiles + t + 1, :] = jnp.sum(new * query, axis=0, keepdims=True)
    readout = ro[...]
    gated = readout * norm_scale(readout) * gain_ref[...] * unit
    read_ref[...] = gated[:, SLOTS // 2 :, :].astype(BF16).astype(F32)


def output_kernel(read_ref, w_ref, out_ref, *, parts, tiles):
    first = 3 * tiles - SLOTS // 2
    rows = jnp.concatenate([read_ref[:, first + t, :] for t in range(tiles)], axis=-1)
    part = jnp.dot(rows.astype(BF16), w_ref[...], preferred_element_type=F32).astype(BF16)
    for s in range(parts):
        out_ref[s] = part


def mixer_kernel(part_ref, x_ref, gain_ref, wg_ref, wu_ref, hid_ref, res_ref, *, parts):
    total = part_ref[0].astype(F32)
    for s in range(1, parts):
        total = total + part_ref[s].astype(F32)
    residual = (wide_rows(x_ref, parts).astype(F32) + total).astype(BF16)
    share = x_ref.shape[2]
    for s in range(parts):
        res_ref[s] = residual[:, s * share : (s + 1) * share]
    wide = residual.astype(F32)
    scale = norm_scale(wide)
    normed = (wide * gain_ref[...]).astype(BF16)
    nt = (((1,), (1,)), ((), ()))
    gate = lax.dot_general(normed, wg_ref[...], nt, preferred_element_type=F32) * scale
    up = lax.dot_general(normed, wu_ref[...], nt, preferred_element_type=F32) * scale
    hidden = (silu(gate) * up).astype(BF16)
    for s in range(parts):
        hid_ref[s] = hidden


def down_kernel(place_ref, hid_ref, res_ref, w_ref, out_ref, *, parts):
    units = hid_ref.shape[2]
    total = res_ref[place_ref[0]].astype(F32)
    for s in range(parts):
        total = total + jnp.dot(
            hid_ref[s], w_ref[s * units : (s + 1) * units, :], preferred_element_type=F32
        )
    out_ref[...] = total.astype(BF16)


def fast_body(
    tokens, old_state, mixer_gain, w_query, w_key, w_value, w_outgate, w_decay, w_write,
    decay_log, decay_bias, head_gain, w_output, channel_gain, w_gate, w_up, w_down, *, parts,
):
    rows, share = tokens.shape
    width = share * parts
    heads = old_state.shape[1]
    tiles = share // HEAD_DIM
    units = w_gate.shape[1]
    shape = jax.ShapeDtypeStruct
    place = lax.axis_index("kv").astype(jnp.int32).reshape(1)
    smem = pl.BlockSpec(memory_space=pltpu.SMEM)
    vmem = pl.BlockSpec(memory_space=pltpu.VMEM)

    tokens, place = lax.optimization_barrier((tokens, place))
    copies = call(
        functools.partial(spread_kernel, parts=parts),
        shape((parts, rows, share), BF16),
        (tokens,),
    )
    x = exchange(copies)
    slab, retain, strength = call(
        functools.partial(project_kernel, parts=parts, tiles=tiles),
        (
            shape((rows, SLOTS, HEAD_DIM), BF16),
            shape((heads, rows), F32),
            shape((heads, rows), F32),
        ),
        (
            x, mixer_gain.reshape(1, width), w_query, w_key, w_value, w_outgate,
            w_decay.T, w_write.T, decay_log.reshape(1, heads), decay_bias.reshape(1, heads),
        ),
        scratch=[pltpu.VMEM((rows, SLOTS, HEAD_DIM), F32)],
    )
    slab = exchange(slab)
    read, new_state = call(
        functools.partial(state_kernel, parts=parts, tiles=tiles),
        (shape((parts, SLOTS // 2, HEAD_DIM), F32), shape((heads, HEAD_DIM, HEAD_DIM), F32)),
        (place, slab, old_state[0], retain, strength, head_gain.reshape(1, HEAD_DIM)),
        scratch=[pltpu.VMEM((parts, SLOTS, HEAD_DIM), F32)],
        spaces=[smem] + [vmem] * 5,
    )
    read = exchange(read)
    part = call(
        functools.partial(output_kernel, parts=parts, tiles=tiles),
        shape((parts, rows, width), BF16),
        (read, w_output),
    )
    part = exchange(part)
    hidden, residual = call(
        functools.partial(mixer_kernel, parts=parts),
        (shape((parts, rows, units), BF16), shape((parts, rows, share), BF16)),
        (part, x, channel_gain.reshape(1, width), w_gate.T, w_up.T),
    )
    hidden = exchange(hidden)
    mixed = call(
        functools.partial(down_kernel, parts=parts),
        shape((rows, share), BF16),
        (place, hidden, residual, w_down),
        spaces=[smem] + [vmem] * 3,
    )
    return mixed, new_state[None]


def body(
    tokens, old_state, mixer_gain, w_query, w_key, w_value, w_outgate, w_decay, w_write,
    decay_log, decay_bias, head_gain, w_output, channel_gain, w_gate, w_up, w_down, *, parts,
):
    rows, share = tokens.shape
    width = share * parts
    local_rows, heads = old_state.shape[:2]
    head_cols = w_query.shape[1]
    place = lax.axis_index("kv")

    tok_wide = gather_kv(tokens, parts).transpose(1, 0, 2).reshape(rows, width).astype(F32)
    scale_in = norm_scale(tok_wide)
    normed = (tok_wide * mixer_gain).astype(BF16)

    def project(weight):
        return (jnp.dot(normed, weight, preferred_element_type=F32) * scale_in).astype(BF16)

    packed = jnp.stack([project(w) for w in (w_query, w_key, w_value, w_outgate)], axis=1)
    packed = exchange(packed.reshape(parts, local_rows, 4, head_cols))

    own_normed = lax.dynamic_slice_in_dim(normed, place * local_rows, local_rows, 0)
    own_scale = lax.dynamic_slice_in_dim(scale_in, place * local_rows, local_rows, 0)
    decay_pre = jnp.dot(own_normed, w_decay, preferred_element_type=F32) * own_scale
    write_pre = jnp.dot(own_normed, w_write, preferred_element_type=F32) * own_scale

    def by_head(index):
        chosen = packed[:, :, index].transpose(1, 0, 2)
        return chosen.reshape(local_rows, heads, HEAD_DIM).astype(F32)

    queries = unit_rows(jax.nn.silu(by_head(0))) * HEAD_DIM ** (-0.5)
    keys_unit = unit_rows(jax.nn.silu(by_head(1)))
    values_act = jax.nn.silu(by_head(2))
    strength = jax.nn.sigmoid(write_pre)
    retain = jnp.exp(-jnp.exp(decay_log) * jax.nn.softplus(decay_pre + decay_bias))
    recalled = jnp.einsum("bhkv,bhk->bhv", old_state, keys_unit, precision=lax.Precision.HIGHEST)
    correction = values_act - retain[..., None] * recalled
    new_state = (
        retain[..., None, None] * old_state
        + (strength[..., None] * keys_unit)[..., :, None] * correction[..., None, :]
    )
    readout = jnp.einsum("bhkv,bhk->bhv", new_state, queries, precision=lax.Precision.HIGHEST)
    gated_read = readout * norm_scale(readout) * head_gain * jax.nn.silu(by_head(3))
    gated_read = gated_read.reshape(local_rows, parts, head_cols).astype(BF16)
    read_cols = exchange(gated_read.transpose(1, 0, 2)).reshape(rows, head_cols)

    partial_out = jnp.dot(read_cols, w_output, preferred_element_type=F32)
    mixer_out = exchange(partial_out.reshape(rows, parts, share).transpose(1, 0, 2)).sum(0)
    own_residual = (tokens.astype(F32) + mixer_out).astype(BF16)
    residual = gather_kv(own_residual, parts).transpose(1, 0, 2).reshape(rows, width)
    residual_wide = residual.astype(F32)
    scale_mid = norm_scale(residual_wide)
    normed_mid = (residual_wide * channel_gain).astype(BF16)
    gate_act = jnp.dot(normed_mid, w_gate, preferred_element_type=F32) * scale_mid
    upward = jnp.dot(normed_mid, w_up, preferred_element_type=F32) * scale_mid
    hidden = (jax.nn.silu(gate_act) * upward).astype(BF16)
    hidden = gather_kv(hidden, parts).transpose(1, 0, 2).reshape(rows, -1)
    down_sum = jnp.dot(hidden, w_down, preferred_element_type=F32)
    mixed = (own_residual.astype(F32) + down_sum).astype(BF16)
    return (mixed, new_state)


def solution(mesh):
    parts = mesh.shape["kv"]
    rows, states = P(("tp", "dp"), "kv"), P(("tp", "dp", "kv"), None, None, None)
    cols = P(None, "kv")
    in_specs = (rows, states, P(), cols, cols, cols, cols, P(), P(), P(), P(), P())
    in_specs += (P("kv", None), P(), cols, cols, cols)

    def step(*args):
        tokens, old_state = args[:2]
        share = tokens.shape[1]
        fits = (
            share % HEAD_DIM == 0
            and 4 * (share // HEAD_DIM) <= SLOTS
            and 3 * (share // HEAD_DIM) >= SLOTS // 2
            and old_state.shape[0] == 1
            and tokens.shape[0] == parts == 8
            and args[3].shape[1] == share
            and args[14].shape[1] % 16 == 0
        )
        return (fast_body if fits else body)(*args, parts=parts)

    return jax.shard_map(
        step, mesh=mesh, in_specs=in_specs, out_specs=(rows, states), check_vma=False
    )
```

time: 96.6 us -> 66.4 us (0.69)
  blocking collectives: 29.7 us -> 55.1 us
  matrix products: 23.5 us -> 0 us
  starting transfers between devices: 14 us -> 0 us
  waiting for transfers between devices: 13.9 us -> 0 us
  local copies, waits for them, and re-layouts: 10.9 us -> 0.77 us
  Pallas kernels: 0 us -> 9.33 us
  other arithmetic: 3.04 us -> 0.01 us
    all_to_all x3 -> x5, blocking collectives: 29.7 us -> 55.1 us  [exchange(): return lax.all_to_all(slabs, 'kv', split_axis=0, concat_axis=0, tiled=True)]
    dot_general x12 -> x0, matrix products: 23.5 us -> none  [the longest x1 4.64 us: body(): upward = jnp.dot(normed_mid, w_up, preferred_element_type=f32) * scale_mid]
    all_to_all x3 -> x0, starting transfers between devices: 14 us -> none  [the longest x1 7.31 us: gather_kv(): return lax.all_to_all(copies, 'kv', split_axis=0, concat_axis=0, tiled=True)]
    all_to_all x3 -> x0, waiting for transfers between devices: 13.9 us -> none  [the longest x1 6.8 us: gather_kv(): return lax.all_to_all(copies, 'kv', split_axis=0, concat_axis=0, tiled=True)]
    pallas_call x0 -> x6, Pallas kernels: none -> 9.33 us  [call(): pl.pallas_call(kernel, out_shape=out_shape, in_specs=specs, out_specs=[vm...]
    dot_general x1 -> x0, local copies, waits for them, and re-layouts: 4.3 us -> none  [body(): partial_out = jnp.dot(read_cols, w_output, preferred_element_type=f32)]
    unnamed x28 -> x40, local copies, waits for them, and re-layouts: 3.18 us -> 0.77 us
    convert_element_type x7 -> x0, other arithmetic: 1.54 us -> none  [the longest x2 0.75 us: body(): gated_read.reshape(local_rows, parts, head_cols).astype(bf16)]
  transfers between devices with their start and end apart: 3 -> 0, of which waited for: 3 -> 0; matrix products, arithmetic and copies ran while one was open for 6% -> 0% of each run, Pallas kernels for 0% -> 0%
where the time goes in v2:
time: 66.4 us; the launch traced here: 66 us
  blocking collectives  55.1 us (83%)
  Pallas kernels  9.33 us (14%)
  between operations  0.85 us (1%)
  local copies, waits for them, and re-layouts  0.77 us (1%)
    all_to_all x5, blocking collectives, exchange(): return lax.all_to_all(slabs, 'kv', split_axis=0, concat_axis=0, tiled=True)  55.1 us
    pallas_call x6, Pallas kernels, call(): pl.pallas_call(kernel, out_shape=out_shape, in_specs=specs, out_specs=[vm...  9.33 us

profile of v2, /device:TPU:0, one launch (start us, length us, event | category | flops | bytes accessed | tf_op | source)
XLA Modules:
  0.0 66.0 jit_solution(6129097693384743585)
XLA Ops:
  0.6 0.0 copy-start.10
  0.6 0.7 %copy-done.10 = bf16[8,384]{1,0:T(8,128)(2,1)S(1)} copy-done((bf16[8,384]{1,0:T(8,128)(2,1)S(1)}, bf16[8,384]{1,0:T(8,128)(2,1)}, u32[]{:S(2)}) %copy-start.10) | copy-done | bytes 6168
  1.3 0.0 copy-start
  1.3 0.0 copy-start.1
  1.3 0.0 copy-start.2
  1.3 0.0 copy-start.3
  1.3 0.0 copy-start.6
  1.4 0.0 copy-start.7
  1.4 0.0 copy-start.8
  1.4 0.0 copy-start.11
  1.4 0.0 copy-start.12
  1.4 14.2 %all_to_all.25.x_ref = bf16[8,8,384]{2,1,0:T(8,128)(2,1)S(1)} all-to-all(bf16[8,8,384]{2,1,0:T(8,128)(2,1)S(1)} %shard_map.176), channel_id=1, replica_groups=mesh['dp'=2,'kv'=8,'tp'=2] {'kv'}, dimensions={0} | all-to-all | bytes 98304 | tf_op jit(solution)/shard_map/all_to_all | solution.py:31
  15.6 0.0 copy-done
  15.6 0.0 copy-done.1
  15.6 0.0 copy-done.2
  15.6 0.0 copy-done.3
  15.6 0.0 copy-done.6
  15.6 0.0 copy-done.7
  15.6 0.0 copy-done.8
  15.6 0.0 copy-done.11
  15.6 0.0 copy-done.12
  15.6 0.0 copy-start.5
  15.7 0.0 copy-start.13
  15.7 1.5 %shard_map.177 = (bf16[8,16,128]{2,1,0:T(8,128)(2,1)S(1)}, f32[24,8]{1,0:T(8,128)S(1)}, f32[24,8]{1,0:T(8,128)S(1)}) custom-call(bf16[8,8,384]{2,1,0:T(8,128)(2,1)S(1)} %all_to_all.25.x_ref, f32[1,3072]{1,0:T(1,128)S(1)} %bitcast.23, bf16[3072,384]{1,0:T(8,128)(2,1)S(1)} %copy-done, bf16[3072,384]{1,0:T(8,128)(2,1)S(1)} %copy-done.1, ...), custom_call_target="tpu_custom_call" | custom-call | flops 4000000000 | bytes 24000000 | tf_op jit(solution)/shard_map/pallas_call | solution.py:42
  17.2 9.1 %all_to_all.26.slab_ref = bf16[8,16,128]{2,1,0:T(8,128)(2,1)S(1)} all-to-all(bf16[8,16,128]{2,1,0:T(8,128)(2,1)S(1)} %get-tuple-element.13), channel_id=1, replica_groups=mesh['dp'=2,'kv'=8,'tp'=2] {'kv'}, dimensions={0} | all-to-all | bytes 65536 | tf_op jit(solution)/shard_map/all_to_all | solution.py:31
  26.2 0.0 copy-done.5
  26.2 0.0 copy-done.13
  26.2 0.0 copy-start.4
  26.2 0.0 slice-start
  26.3 0.0 slice-start.2
  26.3 2.4 %shard_map.178 = (f32[8,8,128]{2,1,0:T(8,128)S(1)}, f32[24,128,128]{2,1,0:T(8,128)}) custom-call(s32[1]{0:T(128)} %bitcast.place_ref, bf16[8,16,128]{2,1,0:T(8,128)(2,1)S(1)} %all_to_all.26.slab_ref, f32[24,128,128]{2,1,0:T(8,128)S(1)} %bitcast.20, f32[24,8]{1,0:T(8,128)S(1)} %get-tuple-element.14.retain_ref, f32[24,8]{1,0:T(8,128)S(1)} %get-tuple-element.15.strength_ref, ...), custom_call_target="tpu_custom_call" | custom-call | flops 4000000000 | bytes 24000000 | tf_op jit(solution)/shard_map/pallas_call | solution.py:42
  28.6 9.3 %all_to_all.27.read_ref = f32[8,8,128]{2,1,0:T(8,128)S(1)} all-to-all(f32[8,8,128]{2,1,0:T(8,128)S(1)} %get-tuple-element.16), channel_id=1, replica_groups=mesh['dp'=2,'kv'=8,'tp'=2] {'kv'}, dimensions={0} | all-to-all | bytes 65536 | tf_op jit(solution)/shard_map/all_to_all | solution.py:31
  37.9 0.0 copy-done.4
  38.0 0.0 slice-start.1
  38.0 0.0 slice-start.3
  38.0 0.4 shard_map.179
  38.4 12.2 %all_to_all.28.part_ref = bf16[8,8,3072]{2,1,0:T(8,128)(2,1)S(1)} all-to-all(bf16[8,8,3072]{2,1,0:T(8,128)(2,1)S(1)} %shard_map.179), channel_id=1, replica_groups=mesh['dp'=2,'kv'=8,'tp'=2] {'kv'}, dimensions={0} | all-to-all | bytes 786432 | tf_op jit(solution)/shard_map/all_to_all | solution.py:31
  50.6 0.0 slice-done
  50.6 0.0 slice-done.2
  50.6 0.0 slice-done.1
  50.6 0.0 slice-done.3
  50.6 0.0 copy-done.9
  50.7 0.0 slice-start.5
  50.7 3.5 %shard_map.180 = (bf16[8,8,1056]{2,1,0:T(8,128)(2,1)S(1)}, bf16[8,8,384]{2,1,0:T(8,128)(2,1)S(1)}) custom-call(bf16[8,8,3072]{2,1,0:T(8,128)(2,1)S(1)} %all_to_all.28.part_ref, bf16[8,8,384]{2,1,0:T(8,128)(2,1)S(1)} %all_to_all.25.x_ref, f32[1,3072]{1,0:T(1,128)S(1)} %bitcast.24, bf16[1056,3072]{1,0:T(8,128)(2,1)S(1)} %bitcast.14, ...), custom_call_target="tpu_custom_call" | custom-call | flops 4000000000 | bytes 24000000 | tf_op jit(solution)/shard_map/pallas_call | solution.py:42
  54.1 10.3 %all_to_all.29.hid_ref = bf16[8,8,1056]{2,1,0:T(8,128)(2,1)S(1)} all-to-all(bf16[8,8,1056]{2,1,0:T(8,128)(2,1)S(1)} %get-tuple-element.17), channel_id=1, replica_groups=mesh['dp'=2,'kv'=8,'tp'=2] {'kv'}, dimensions={0} | all-to-all | bytes 270336 | tf_op jit(solution)/shard_map/all_to_all | solution.py:31
  64.4 0.0 slice-done.4
  64.4 0.0 slice-done.5
  64.4 1.6 %shard_map.181 = bf16[8,384]{1,0:T(8,128)(2,1)} custom-call(s32[1]{0:T(128)} %bitcast.place_ref, bf16[8,8,1056]{2,1,0:T(8,128)(2,1)S(1)} %all_to_all.29.hid_ref, bf16[8,8,384]{2,1,0:T(8,128)(2,1)S(1)} %get-tuple-element.18.res_ref, bf16[8448,384]{1,0:T(8,128)(2,1)S(1)} %bitcast.19), custom_call_target="tpu_custom_call" | custom-call | flops 4000000000 | bytes 24000000 | tf_op jit(solution)/shard_map/pallas_call | solution.py:42
  (6 shorter events, 0.0 us)
Async XLA Ops:
  0.6 0.7 %copy-start.10 = (bf16[8,384]{1,0:T(8,128)(2,1)S(1)}, bf16[8,384]{1,0:T(8,128)(2,1)}, u32[]{:S(2)}) copy-start(bf16[8,384]{1,0:T(8,128)(2,1)} %block_ref) | copy-start | bytes 18436
  1.3 14.2 %copy-start = (bf16[3072,384]{1,0:T(8,128)(2,1)S(1)}, bf16[3072,384]{1,0:T(8,128)(2,1)}, u32[]{:S(2)}) copy-start(bf16[3072,384]{1,0:T(8,128)(2,1)} %wq.1) | copy-start | bytes 7077892
  1.3 14.2 %copy-start.1 = (bf16[3072,384]{1,0:T(8,128)(2,1)S(1)}, bf16[3072,384]{1,0:T(8,128)(2,1)}, u32[]{:S(2)}) copy-start(bf16[3072,384]{1,0:T(8,128)(2,1)} %wk.1) | copy-start | bytes 7077892
  1.3 14.2 %copy-start.2 = (bf16[3072,384]{1,0:T(8,128)(2,1)S(1)}, bf16[3072,384]{1,0:T(8,128)(2,1)}, u32[]{:S(2)}) copy-start(bf16[3072,384]{1,0:T(8,128)(2,1)} %wv.1) | copy-start | bytes 7077892
  1.3 14.2 %copy-start.3 = (bf16[3072,384]{1,0:T(8,128)(2,1)S(1)}, bf16[3072,384]{1,0:T(8,128)(2,1)}, u32[]{:S(2)}) copy-start(bf16[3072,384]{1,0:T(8,128)(2,1)} %wg.1) | copy-start | bytes 7077892
  1.3 14.3 %copy-start.6 = (bf16[3072,24]{0,1:T(8,128)(2,1)S(1)}, bf16[3072,24]{0,1:T(8,128)(2,1)}, u32[]{:S(2)}) copy-start(bf16[3072,24]{0,1:T(8,128)(2,1)} %param.24) | copy-start | bytes 442372
  1.4 14.3 %copy-start.7 = (bf16[3072,24]{0,1:T(8,128)(2,1)S(1)}, bf16[3072,24]{0,1:T(8,128)(2,1)}, u32[]{:S(2)}) copy-start(bf16[3072,24]{0,1:T(8,128)(2,1)} %param.25) | copy-start | bytes 442372
  1.4 14.3 %copy-start.8 = (f32[3072]{0:T(1024)S(1)}, f32[3072]{0:T(1024)}, u32[]{:S(2)}) copy-start(f32[3072]{0:T(1024)} %param.19) | copy-start | bytes 36868
  1.4 14.3 %copy-start.11 = (f32[24]{0:T(128)S(1)}, f32[24]{0:T(128)}, u32[]{:S(2)}) copy-start(f32[24]{0:T(128)} %param.26) | copy-start | bytes 292
  1.4 14.3 %copy-start.12 = (f32[24]{0:T(128)S(1)}, f32[24]{0:T(128)}, u32[]{:S(2)}) copy-start(f32[24]{0:T(128)} %param.27) | copy-start | bytes 292
  15.6 10.6 %copy-start.5 = (f32[1,24,128,128]{3,2,1,0:T(8,128)S(1)}, f32[1,24,128,128]{3,2,1,0:T(8,128)}, u32[]{:S(2)}) copy-start(f32[1,24,128,128]{3,2,1,0:T(8,128)} %param.18) | copy-start | bytes 4718596
  15.7 10.6 %copy-start.13 = (f32[128]{0:T(128)S(1)}, f32[128]{0:T(128)}, u32[]{:S(2)}) copy-start(f32[128]{0:T(128)} %param.28) | copy-start | bytes 1540
  26.2 11.7 %copy-start.4 = (bf16[384,3072]{1,0:T(8,128)(2,1)S(1)}, bf16[384,3072]{1,0:T(8,128)(2,1)}, u32[]{:S(2)}) copy-start(bf16[384,3072]{1,0:T(8,128)(2,1)} %w_ref.2) | copy-start | bytes 7077892
  26.2 24.4 %slice-start = ((s8[6488064]{0:T(1024)(128)(4,1)}), s8[4194304]{0:T(1024)(128)(4,1)S(1)}, s32[]{:S(2)}) async-start(s8[6488064]{0:T(1024)(128)(4,1)} %bitcast.12), calls=%async_computation.5 | async-start | bytes 8388608
  26.3 24.4 %slice-start.2 = ((s8[6488064]{0:T(1024)(128)(4,1)}), s8[4194304]{0:T(1024)(128)(4,1)S(1)}, s32[]{:S(2)}) async-start(s8[6488064]{0:T(1024)(128)(4,1)} %bitcast.15), calls=%async_computation.7 | async-start | bytes 8388608
  38.0 12.7 %slice-start.1 = ((s8[6488064]{0:T(1024)(128)(4,1)}), s8[2293760]{0:T(1024)(128)(4,1)S(1)}, s32[]{:S(2)}) async-start(s8[6488064]{0:T(1024)(128)(4,1)} %bitcast.12), calls=%async_computation.6 | async-start | bytes 4587520
  38.0 12.7 %slice-start.3 = ((s8[6488064]{0:T(1024)(128)(4,1)}), s8[2293760]{0:T(1024)(128)(4,1)S(1)}, s32[]{:S(2)}) async-start(s8[6488064]{0:T(1024)(128)(4,1)} %bitcast.15), calls=%async_computation.8 | async-start | bytes 4587520
  38.0 12.7 %copy-start.9 = (f32[3072]{0:T(1024)S(1)}, f32[3072]{0:T(1024)}, u32[]{:S(2)}) copy-start(f32[3072]{0:T(1024)} %param.30) | copy-start | bytes 36868
  38.4 26.1 %slice-start.4 = ((s8[6488064]{0:T(1024)(128)(4,1)}), s8[4194304]{0:T(1024)(128)(4,1)S(1)}, s32[]{:S(2)}) async-start(s8[6488064]{0:T(1024)(128)(4,1)} %bitcast.18), calls=%async_computation.9 | async-start | bytes 8388608
  50.7 13.8 %slice-start.5 = ((s8[6488064]{0:T(1024)(128)(4,1)}), s8[2293760]{0:T(1024)(128)(4,1)S(1)}, s32[]{:S(2)}) async-start(s8[6488064]{0:T(1024)(128)(4,1)} %bitcast.18), calls=%async_computation.10 | async-start | bytes 4587520

commit v3 on v2

v3 whole, which is shorter than its diff:
```python
import functools

import jax
import jax.numpy as jnp
from jax import lax
from jax.experimental import pallas as pl
from jax.experimental.pallas import tpu as pltpu
from jax.sharding import PartitionSpec as P

HEAD_DIM = 128
EPS = 1e-06
MIB = 1 << 20

F32, BF16 = jnp.float32, jnp.bfloat16


def norm_scale(values):
    return lax.rsqrt(jnp.mean(values * values, axis=-1, keepdims=True) + EPS)


def unit_rows(values):
    return values * lax.rsqrt(jnp.sum(values * values, axis=-1, keepdims=True) + EPS)


def silu(values):
    return values / (1.0 + jnp.exp(-values))


def exchange(slabs):
    return lax.all_to_all(slabs, "kv", split_axis=0, concat_axis=0, tiled=True)


def gather_kv(block, parts):
    return exchange(jnp.broadcast_to(block[None], (parts,) + block.shape))


def call(kernel, out_shape, args, *, limit=8, scratch=(), spaces=None, outs=None, span=8):
    vmem = pl.BlockSpec(memory_space=pltpu.VMEM)
    specs = [vmem] * len(args) if spaces is None else spaces
    many = isinstance(out_shape, (tuple, list))
    return pl.pallas_call(
        kernel,
        out_shape=out_shape,
        in_specs=specs,
        out_specs=outs or ([vmem] * len(out_shape) if many else vmem),
        scratch_shapes=list(scratch),
        compiler_params=pltpu.CompilerParams(vmem_limit_bytes=limit * MIB),
        cost_estimate=pl.CostEstimate(
            flops=span * 500_000_000, bytes_accessed=span * 3_000_000, transcendentals=0
        ),
    )(*args)


def eye(n):
    across = lax.broadcasted_iota(jnp.int32, (n, n), 1)
    return lax.broadcasted_iota(jnp.int32, (n, n), 0) == across


def upright(row):
    return jnp.sum(jnp.where(eye(row.shape[1]), row, 0.0), axis=1, keepdims=True)


def pack_kernel(tok_ref, s_hbm, out_ref, buf, sems, *, parts, tiles):
    copies = [
        pltpu.make_async_copy(
            s_hbm.at[pl.ds(d * tiles, tiles)], buf.at[pl.ds(d * tiles, tiles)], sems.at[d]
        )
        for d in range(parts)
    ]
    for copy in copies:
        copy.start()
    depth = tiles * HEAD_DIM
    tok = tok_ref[...].astype(F32)
    tok = jnp.concatenate(
        [tok[:, t * HEAD_DIM : (t + 1) * HEAD_DIM] for t in range(tiles)], axis=0
    ).astype(BF16)
    for d in range(parts):
        out_ref[d, depth:, :] = tok
    for d, copy in enumerate(copies):
        copy.wait()
        for t in range(tiles):
            out_ref[d, t * HEAD_DIM : (t + 1) * HEAD_DIM, :] = buf[d * tiles + t].astype(BF16)


def eye(n):
    across = lax.broadcasted_iota(jnp.int32, (n, n), 1)
    return lax.broadcasted_iota(jnp.int32, (n, n), 0) == across


def upright(row):
    return jnp.sum(jnp.where(eye(row.shape[1]), row, 0.0), axis=1, keepdims=True)


def wide_tokens(x_ref, *, parts, tiles):
    depth = tiles * HEAD_DIM
    rows = (x_ref.shape[1] - depth) // tiles
    pieces = []
    for s in range(parts):
        tok = x_ref[s, depth:, :].astype(F32)
        pieces += [tok[t * rows : (t + 1) * rows, :] for t in range(tiles)]
    return jnp.concatenate(pieces, axis=-1)


def heads_kernel(
    place_ref, x_ref, gain_ref, wq, wk, wv, wg, wd_ref, ww_ref, log_ref, bias_ref,
    head_gain_ref, wo_ref, out_ref, retain_ref, strength_ref, kv, *, parts, tiles,
):
    nt = (((1,), (1,)), ((), ()))
    place = place_ref[0]
    x = wide_tokens(x_ref, parts=parts, tiles=tiles)
    rows, width = x.shape
    scale = norm_scale(x)
    normed = (x * gain_ref[...]).astype(BF16)

    decay = lax.dot_general(normed, wd_ref[...], nt, preferred_element_type=F32) * scale
    write = lax.dot_general(normed, ww_ref[...], nt, preferred_element_type=F32) * scale
    pre = decay + bias_ref[...]
    soft = jnp.maximum(pre, 0.0) + jnp.log1p(jnp.exp(-jnp.abs(pre)))
    retain_all = jnp.exp(-jnp.exp(log_ref[...]) * soft)
    strength_all = 1.0 / (1.0 + jnp.exp(-write))
    retain_ref[...] = retain_all
    strength_ref[...] = strength_all
    head = lax.broadcasted_iota(jnp.int32, retain_all.shape, 1)

    def project(w):
        acc = jnp.dot(normed, w[...], preferred_element_type=F32) * scale
        return acc.astype(BF16).astype(F32)

    query_pre, key_pre, value_pre, gate_pre = project(wq), project(wk), project(wv), project(wg)
    row = lax.broadcasted_iota(jnp.int32, (rows, HEAD_DIM), 0)
    kv[2 * tiles :] = jnp.zeros((kv.shape[0] - 2 * tiles, rows, HEAD_DIM), F32)
    gated = []
    for t in range(tiles):
        lanes = slice(t * HEAD_DIM, (t + 1) * HEAD_DIM)
        kv[t] = key_pre[:, lanes]
        kv[tiles + t] = value_pre[:, lanes]
        query = unit_rows(silu(query_pre[:, lanes])) * HEAD_DIM ** (-0.5)
        key = unit_rows(silu(key_pre[:, lanes]))
        value = silu(value_pre[:, lanes])
        own = head == place * tiles + t
        retain = jnp.sum(jnp.where(own, retain_all, 0.0), axis=1, keepdims=True)
        strength = jnp.sum(jnp.where(own, strength_all, 0.0), axis=1, keepdims=True)
        stack = []
        for vector in (key, query):
            high = vector.astype(BF16).astype(F32)
            stack += [high, vector - high]
        stack = jnp.concatenate(stack, axis=0).astype(BF16)
        found = [jnp.zeros((rows, HEAD_DIM), F32)] * 2
        for r in range(rows):
            product = jnp.dot(
                stack, x_ref[r, t * HEAD_DIM : (t + 1) * HEAD_DIM, :], preferred_element_type=F32
            )
            for i in range(2):
                both = product[2 * i * rows : (2 * i + 1) * rows] + product[
                    (2 * i + 1) * rows : (2 * i + 2) * rows
                ]
                found[i] = jnp.where(row == r, both, found[i])
        correction = value - retain * found[0]
        along = jnp.sum(key * query, axis=-1, keepdims=True)
        readout = retain * found[1] + (strength * along) * correction
        gated.append(
            readout * norm_scale(readout) * head_gain_ref[...] * silu(gate_pre[:, lanes])
        )
    gated = jnp.concatenate(gated, axis=-1).astype(BF16)
    part = jnp.dot(gated, wo_ref[...], preferred_element_type=F32).astype(BF16)
    for d in range(parts):
        out_ref[d, :, :width] = part
        out_ref[d, :, width:] = kv[:, d, :].astype(BF16)


def mixer_kernel(
    place_ref, part_ref, x_ref, gain_ref, retain_ref, strength_ref, s_ref, wg_ref, wu_ref,
    hid_ref, res_ref, new_hbm, new, sems, *, parts, tiles,
):
    nt = (((1,), (1,)), ((), ()))
    place = place_ref[0]
    width = gain_ref.shape[1]
    share = width // parts
    pre = jnp.concatenate([part_ref[j, :, width:].astype(F32) for j in range(parts)], axis=0)
    act = silu(pre)
    columns = unit_rows(act).T
    retain = jnp.broadcast_to(upright(retain_ref[pl.ds(place, 1), :]), (parts * tiles, HEAD_DIM))
    strength = jnp.broadcast_to(
        upright(strength_ref[pl.ds(place, 1), :]), (parts * tiles, HEAD_DIM)
    )
    slots = part_ref.shape[1]
    copies = []
    for j in range(parts):
        for t in range(tiles):
            h = j * tiles + t
            base = j * slots + t
            key = columns[:, base : base + 1]
            value = act[base + tiles : base + tiles + 1, :]
            old = s_ref[h]
            keep = retain[h : h + 1, :]
            recalled = jnp.sum(old * key, axis=0, keepdims=True)
            correction = (value - keep * recalled) * strength[h : h + 1, :]
            new[h] = keep * old + key * correction
        copies.append(
            pltpu.make_async_copy(
                new.at[pl.ds(j * tiles, tiles)], new_hbm.at[pl.ds(j * tiles, tiles)], sems.at[j]
            )
        )
        copies[-1].start()

    total = part_ref[0, :, :width].astype(F32)
    for s in range(1, parts):
        total = total + part_ref[s, :, :width].astype(F32)
    residual = (wide_tokens(x_ref, parts=parts, tiles=tiles) + total).astype(BF16)
    for s in range(parts):
        res_ref[s] = residual[:, s * share : (s + 1) * share]
    wide = residual.astype(F32)
    scale = norm_scale(wide)
    normed = (wide * gain_ref[...]).astype(BF16)
    gate = lax.dot_general(normed, wg_ref[...], nt, preferred_element_type=F32) * scale
    up = lax.dot_general(normed, wu_ref[...], nt, preferred_element_type=F32) * scale
    hidden = (silu(gate) * up).astype(BF16)
    for s in range(parts):
        hid_ref[s] = hidden
    for copy in copies:
        copy.wait()


def down_kernel(place_ref, hid_ref, res_ref, w_ref, out_ref, *, parts):
    units = hid_ref.shape[2]
    total = res_ref[place_ref[0]].astype(F32)
    for s in range(parts):
        total = total + jnp.dot(
            hid_ref[s], w_ref[s * units : (s + 1) * units, :], preferred_element_type=F32
        )
    out_ref[...] = total.astype(BF16)


def fast_body(
    tokens, old_state, mixer_gain, w_query, w_key, w_value, w_outgate, w_decay, w_write,
    decay_log, decay_bias, head_gain, w_output, channel_gain, w_gate, w_up, w_down, *, parts,
):
    rows, share = tokens.shape
    width = share * parts
    heads = old_state.shape[1]
    tiles = share // HEAD_DIM
    units = w_gate.shape[1]
    shape = jax.ShapeDtypeStruct
    place = lax.axis_index("kv").astype(jnp.int32).reshape(1)
    smem = pl.BlockSpec(memory_space=pltpu.SMEM)
    vmem = pl.BlockSpec(memory_space=pltpu.VMEM)
    hbm = pl.BlockSpec(memory_space=pltpu.HBM)
    states = (heads, HEAD_DIM, HEAD_DIM)
    state = old_state[0]

    tokens, place = lax.optimization_barrier((tokens, place))
    slabs = call(
        functools.partial(pack_kernel, parts=parts, tiles=tiles),
        shape((parts, tiles * (HEAD_DIM + rows), HEAD_DIM), BF16),
        (tokens, state),
        scratch=[pltpu.VMEM(states, F32), pltpu.SemaphoreType.DMA((parts,))],
        spaces=[vmem, hbm],
    )
    x = exchange(slabs)
    part, retain, strength = call(
        functools.partial(heads_kernel, parts=parts, tiles=tiles),
        (
            shape((parts, rows, width + HEAD_DIM), BF16),
            shape((rows, heads), F32),
            shape((rows, heads), F32),
        ),
        (
            place, x, mixer_gain.reshape(1, width), w_query, w_key, w_value, w_outgate,
            w_decay.T, w_write.T, decay_log.reshape(1, heads), decay_bias.reshape(1, heads),
            head_gain.reshape(1, HEAD_DIM), w_output,
        ),
        scratch=[pltpu.VMEM((rows, rows, HEAD_DIM), F32)],
        spaces=[smem] + [vmem] * 12,
    )
    part = exchange(part)
    hidden, residual, new_state = call(
        functools.partial(mixer_kernel, parts=parts, tiles=tiles),
        (
            shape((parts, rows, units), BF16),
            shape((parts, rows, share), BF16),
            shape(states, F32),
        ),
        (
            place, part, x, channel_gain.reshape(1, width), retain, strength, state,
            w_gate.T, w_up.T,
        ),
        scratch=[pltpu.VMEM(states, F32), pltpu.SemaphoreType.DMA((parts,))],
        spaces=[smem] + [vmem] * 8,
        outs=[vmem, vmem, hbm],
    )
    hidden = exchange(hidden)
    mixed = call(
        functools.partial(down_kernel, parts=parts),
        shape((rows, share), BF16),
        (place, hidden, residual, w_down),
        spaces=[smem] + [vmem] * 3,
    )
    return mixed, new_state[None]


def body(
    tokens, old_state, mixer_gain, w_query, w_key, w_value, w_outgate, w_decay, w_write,
    decay_log, decay_bias, head_gain, w_output, channel_gain, w_gate, w_up, w_down, *, parts,
):
    rows, share = tokens.shape
    width = share * parts
    local_rows, heads = old_state.shape[:2]
    head_cols = w_query.shape[1]
    place = lax.axis_index("kv")

    tok_wide = gather_kv(tokens, parts).transpose(1, 0, 2).reshape(rows, width).astype(F32)
    scale_in = norm_scale(tok_wide)
    normed = (tok_wide * mixer_gain).astype(BF16)

    def project(weight):
        return (jnp.dot(normed, weight, preferred_element_type=F32) * scale_in).astype(BF16)

    packed = jnp.stack([project(w) for w in (w_query, w_key, w_value, w_outgate)], axis=1)
    packed = exchange(packed.reshape(parts, local_rows, 4, head_cols))

    own_normed = lax.dynamic_slice_in_dim(normed, place * local_rows, local_rows, 0)
    own_scale = lax.dynamic_slice_in_dim(scale_in, place * local_rows, local_rows, 0)
    decay_pre = jnp.dot(own_normed, w_decay, preferred_element_type=F32) * own_scale
    write_pre = jnp.dot(own_normed, w_write, preferred_element_type=F32) * own_scale

    def by_head(index):
        chosen = packed[:, :, index].transpose(1, 0, 2)
        return chosen.reshape(local_rows, heads, HEAD_DIM).astype(F32)

    queries = unit_rows(jax.nn.silu(by_head(0))) * HEAD_DIM ** (-0.5)
    keys_unit = unit_rows(jax.nn.silu(by_head(1)))
    values_act = jax.nn.silu(by_head(2))
    strength = jax.nn.sigmoid(write_pre)
    retain = jnp.exp(-jnp.exp(decay_log) * jax.nn.softplus(decay_pre + decay_bias))
    recalled = jnp.einsum("bhkv,bhk->bhv", old_state, keys_unit, precision=lax.Precision.HIGHEST)
    correction = values_act - retain[..., None] * recalled
    new_state = (
        retain[..., None, None] * old_state
        + (strength[..., None] * keys_unit)[..., :, None] * correction[..., None, :]
    )
    readout = jnp.einsum("bhkv,bhk->bhv", new_state, queries, precision=lax.Precision.HIGHEST)
    gated_read = readout * norm_scale(readout) * head_gain * jax.nn.silu(by_head(3))
    gated_read = gated_read.reshape(local_rows, parts, head_cols).astype(BF16)
    read_cols = exchange(gated_read.transpose(1, 0, 2)).reshape(rows, head_cols)

    partial_out = jnp.dot(read_cols, w_output, preferred_element_type=F32)
    mixer_out = exchange(partial_out.reshape(rows, parts, share).transpose(1, 0, 2)).sum(0)
    own_residual = (tokens.astype(F32) + mixer_out).astype(BF16)
    residual = gather_kv(own_residual, parts).transpose(1, 0, 2).reshape(rows, width)
    residual_wide = residual.astype(F32)
    scale_mid = norm_scale(residual_wide)
    normed_mid = (residual_wide * channel_gain).astype(BF16)
    gate_act = jnp.dot(normed_mid, w_gate, preferred_element_type=F32) * scale_mid
    upward = jnp.dot(normed_mid, w_up, preferred_element_type=F32) * scale_mid
    hidden = (jax.nn.silu(gate_act) * upward).astype(BF16)
    hidden = gather_kv(hidden, parts).transpose(1, 0, 2).reshape(rows, -1)
    down_sum = jnp.dot(hidden, w_down, preferred_element_type=F32)
    mixed = (own_residual.astype(F32) + down_sum).astype(BF16)
    return (mixed, new_state)


def solution(mesh):
    parts = mesh.shape["kv"]
    rows, states = P(("tp", "dp"), "kv"), P(("tp", "dp", "kv"), None, None, None)
    cols = P(None, "kv")
    in_specs = (rows, states, P(), cols, cols, cols, cols, P(), P(), P(), P(), P())
    in_specs += (P("kv", None), P(), cols, cols, cols)

    def step(*args):
        tokens, old_state = args[:2]
        share = tokens.shape[1]
        fits = (
            share % HEAD_DIM == 0
            and 2 * (share // HEAD_DIM) <= tokens.shape[0]
            and old_state.shape[0] == 1
            and tokens.shape[0] == parts == 8
            and args[3].shape[1] == share
            and args[14].shape[1] % 16 == 0
        )
        return (fast_body if fits else body)(*args, parts=parts)

    return jax.shard_map(
        step, mesh=mesh, in_specs=in_specs, out_specs=(rows, states), check_vma=False
    )
```

time: 66.4 us -> 68.4 us (1.030)
  local copies, waits for them, and re-layouts: 0.77 us -> 2.19 us
    unnamed x40 -> x42, local copies, waits for them, and re-layouts: 0.77 us -> 2.19 us
    pallas_call x6 -> x4, Pallas kernels: 9.33 us -> 10 us  [call(): pl.pallas_call(kernel, out_shape=out_shape, in_specs=specs, out_specs=out...]
    all_to_all x5 -> x3, blocking collectives: 55.1 us -> 55 us  [exchange(): return lax.all_to_all(slabs, 'kv', split_axis=0, concat_axis=0, tiled=True)]
where the time goes in v3:
time: 68.4 us; the launch traced here: 68.1 us
  blocking collectives  55 us (80%)
  Pallas kernels  10 us (15%)
  local copies, waits for them, and re-layouts  2.19 us (3%)
  between operations  0.9 us (1%)
    all_to_all x3, blocking collectives, exchange(): return lax.all_to_all(slabs, 'kv', split_axis=0, concat_axis=0, tiled=True)  55 us
    pallas_call x4, Pallas kernels, call(): pl.pallas_call(kernel, out_shape=out_shape, in_specs=specs, out_specs=out...  10 us
    unnamed x42, local copies, waits for them, and re-layouts  2.19 us

profile of v3, /device:TPU:0, one launch (start us, length us, event | category | flops | bytes accessed | tf_op | source)
XLA Modules:
  0.0 68.1 jit_solution(2475041932748660169)
XLA Ops:
  0.6 0.0 copy-start
  0.7 1.4 %copy-done = f32[1,24,128,128]{3,2,1,0:T(8,128)S(1)} copy-done((f32[1,24,128,128]{3,2,1,0:T(8,128)S(1)}, f32[1,24,128,128]{3,2,1,0:T(8,128)}, u32[]{:S(2)}) %copy-start) | copy-done | bytes 1572888
  2.1 0.0 copy-start.11
  2.1 0.7 %copy-done.11 = bf16[8,384]{1,0:T(8,128)(2,1)S(1)} copy-done((bf16[8,384]{1,0:T(8,128)(2,1)S(1)}, bf16[8,384]{1,0:T(8,128)(2,1)}, u32[]{:S(2)}) %copy-start.11) | copy-done | bytes 6168
  2.7 0.0 copy-start.3
  2.7 0.0 copy-start.4
  2.7 0.0 copy-start.5
  2.7 0.0 copy-start.6
  2.8 0.0 copy-start.7
  2.8 0.0 copy-start.8
  2.8 0.0 copy-start.9
  2.8 0.0 copy-start.10
  2.8 0.0 copy-start.12
  2.8 0.0 copy-start.13
  2.8 0.0 copy-start.14
  2.8 0.0 slice-start.2
  2.8 2.2 %shard_map.176 = bf16[8,408,128]{2,1,0:T(8,128)(2,1)S(1)} custom-call(bf16[8,384]{1,0:T(8,128)(2,1)S(1)} %copy-done.11, f32[24,128,128]{2,1,0:T(8,128)S(1)} %bitcast.18), custom_call_target="tpu_custom_call" | custom-call | flops 4000000000 | bytes 24000000 | tf_op jit(solution)/shard_map/pallas_call | solution.py:41
  5.0 0.0 slice-start
  5.1 0.0 slice-start.3
  5.1 29.2 %all_to_all.15.x_ref = bf16[8,408,128]{2,1,0:T(8,128)(2,1)S(1)} all-to-all(bf16[8,408,128]{2,1,0:T(8,128)(2,1)S(1)} %shard_map.176), channel_id=1, replica_groups=mesh['dp'=2,'kv'=8,'tp'=2] {'kv'}, dimensions={0} | all-to-all | bytes 1671168 | tf_op jit(solution)/shard_map/all_to_all | solution.py:30
  34.3 0.0 copy-done.3
  34.3 0.0 copy-done.4
  34.3 0.0 copy-done.5
  34.3 0.0 copy-done.6
  34.3 0.0 copy-done.7
  34.3 0.0 copy-done.8
  34.3 0.0 copy-done.9
  34.4 0.0 copy-done.10
  34.4 0.0 copy-done.12
  34.4 0.0 copy-done.13
  34.4 0.0 copy-done.14
  34.4 0.0 slice-start.1
  34.4 0.0 copy-start.1
  34.4 0.0 copy-start.2
  34.4 2.1 %shard_map.177 = (bf16[8,8,3200]{2,1,0:T(8,128)(2,1)S(1)}, f32[8,24]{1,0:T(8,128)S(1)}, f32[8,24]{1,0:T(8,128)S(1)}) custom-call(s32[1]{0:T(128)} %bitcast.place_ref, bf16[8,408,128]{2,1,0:T(8,128)(2,1)S(1)} %all_to_all.15.x_ref, f32[1,3072]{1,0:T(1,128)S(1)} %bitcast.25, bf16[3072,384]{1,0:T(8,128)(2,1)S(1)} %copy-done.3, bf16[3072,384]{1,0:T(8,128)(2,1)S(1)} %copy-done.4, ...), custom_call_target="tpu_custom_call" | custom-call | flops 4000000000 | bytes 24000000 | tf_op jit(solution)/shard_map/pallas_call | solution.py:41
  36.6 15.3 %all_to_all.16.part_ref = bf16[8,8,3200]{2,1,0:T(8,128)(2,1)S(1)} all-to-all(bf16[8,8,3200]{2,1,0:T(8,128)(2,1)S(1)} %get-tuple-element.12), channel_id=1, replica_groups=mesh['dp'=2,'kv'=8,'tp'=2] {'kv'}, dimensions={0} | all-to-all | bytes 819200 | tf_op jit(solution)/shard_map/all_to_all | solution.py:30
  51.8 0.0 slice-done.2
  51.8 0.0 slice-done
  51.8 0.0 slice-done.3
  51.8 0.0 slice-done.1
  51.8 0.0 copy-done.1
  51.9 0.0 copy-done.2
  51.9 0.0 slice-start.5
  51.9 4.1 %shard_map.178 = (bf16[8,8,1056]{2,1,0:T(8,128)(2,1)S(1)}, bf16[8,8,384]{2,1,0:T(8,128)(2,1)S(1)}, f32[24,128,128]{2,1,0:T(8,128)}) custom-call(s32[1]{0:T(128)} %bitcast.place_ref, bf16[8,8,3200]{2,1,0:T(8,128)(2,1)S(1)} %all_to_all.16.part_ref, bf16[8,408,128]{2,1,0:T(8,128)(2,1)S(1)} %all_to_all.15.x_ref, f32[1,3072]{1,0:T(1,128)S(1)} %bitcast.20, ...), custom_call_target="tpu_custom_call" | custom-call | flops 4000000000 | bytes 24000000 | tf_op jit(solution)/shard_map/pallas_call | solution.py:41
  56.0 10.5 %all_to_all.17.hid_ref = bf16[8,8,1056]{2,1,0:T(8,128)(2,1)S(1)} all-to-all(bf16[8,8,1056]{2,1,0:T(8,128)(2,1)S(1)} %get-tuple-element.15), channel_id=1, replica_groups=mesh['dp'=2,'kv'=8,'tp'=2] {'kv'}, dimensions={0} | all-to-all | bytes 270336 | tf_op jit(solution)/shard_map/all_to_all | solution.py:30
  66.5 0.0 slice-done.4
  66.5 0.0 slice-done.5
  66.5 1.6 %shard_map.179 = bf16[8,384]{1,0:T(8,128)(2,1)} custom-call(s32[1]{0:T(128)} %bitcast.place_ref, bf16[8,8,1056]{2,1,0:T(8,128)(2,1)S(1)} %all_to_all.17.hid_ref, bf16[8,8,384]{2,1,0:T(8,128)(2,1)S(1)} %get-tuple-element.16.res_ref, bf16[8448,384]{1,0:T(8,128)(2,1)S(1)} %bitcast.22), custom_call_target="tpu_custom_call" | custom-call | flops 4000000000 | bytes 24000000 | tf_op jit(solution)/shard_map/pallas_call | solution.py:41
  (4 shorter events, 0.0 us)
Async XLA Ops:
  0.6 1.4 %copy-start = (f32[1,24,128,128]{3,2,1,0:T(8,128)S(1)}, f32[1,24,128,128]{3,2,1,0:T(8,128)}, u32[]{:S(2)}) copy-start(f32[1,24,128,128]{3,2,1,0:T(8,128)} %param.18) | copy-start | bytes 4718596
  2.1 0.7 %copy-start.11 = (bf16[8,384]{1,0:T(8,128)(2,1)S(1)}, bf16[8,384]{1,0:T(8,128)(2,1)}, u32[]{:S(2)}) copy-start(bf16[8,384]{1,0:T(8,128)(2,1)} %tok_ref) | copy-start | bytes 18436
  2.7 31.6 %copy-start.3 = (bf16[3072,384]{1,0:T(8,128)(2,1)S(1)}, bf16[3072,384]{1,0:T(8,128)(2,1)}, u32[]{:S(2)}) copy-start(bf16[3072,384]{1,0:T(8,128)(2,1)} %wq.1) | copy-start | bytes 7077892
  2.7 31.6 %copy-start.4 = (bf16[3072,384]{1,0:T(8,128)(2,1)S(1)}, bf16[3072,384]{1,0:T(8,128)(2,1)}, u32[]{:S(2)}) copy-start(bf16[3072,384]{1,0:T(8,128)(2,1)} %wk.1) | copy-start | bytes 7077892
  2.7 31.6 %copy-start.5 = (bf16[3072,384]{1,0:T(8,128)(2,1)S(1)}, bf16[3072,384]{1,0:T(8,128)(2,1)}, u32[]{:S(2)}) copy-start(bf16[3072,384]{1,0:T(8,128)(2,1)} %wv.1) | copy-start | bytes 7077892
  2.7 31.6 %copy-start.6 = (bf16[3072,384]{1,0:T(8,128)(2,1)S(1)}, bf16[3072,384]{1,0:T(8,128)(2,1)}, u32[]{:S(2)}) copy-start(bf16[3072,384]{1,0:T(8,128)(2,1)} %wg.1) | copy-start | bytes 7077892
  2.8 31.6 %copy-start.7 = (bf16[384,3072]{1,0:T(8,128)(2,1)S(1)}, bf16[384,3072]{1,0:T(8,128)(2,1)}, u32[]{:S(2)}) copy-start(bf16[384,3072]{1,0:T(8,128)(2,1)} %wo_ref.1) | copy-start | bytes 7077892
  2.8 31.6 %copy-start.8 = (bf16[3072,24]{0,1:T(8,128)(2,1)S(1)}, bf16[3072,24]{0,1:T(8,128)(2,1)}, u32[]{:S(2)}) copy-start(bf16[3072,24]{0,1:T(8,128)(2,1)} %param.24) | copy-start | bytes 442372
  2.8 31.6 %copy-start.9 = (bf16[3072,24]{0,1:T(8,128)(2,1)S(1)}, bf16[3072,24]{0,1:T(8,128)(2,1)}, u32[]{:S(2)}) copy-start(bf16[3072,24]{0,1:T(8,128)(2,1)} %param.25) | copy-start | bytes 442372
  2.8 31.6 %copy-start.10 = (f32[3072]{0:T(1024)S(1)}, f32[3072]{0:T(1024)}, u32[]{:S(2)}) copy-start(f32[3072]{0:T(1024)} %param.19) | copy-start | bytes 36868
  2.8 31.6 %copy-start.12 = (f32[24]{0:T(128)S(1)}, f32[24]{0:T(128)}, u32[]{:S(2)}) copy-start(f32[24]{0:T(128)} %param.26) | copy-start | bytes 292
  2.8 31.6 %copy-start.13 = (f32[24]{0:T(128)S(1)}, f32[24]{0:T(128)}, u32[]{:S(2)}) copy-start(f32[24]{0:T(128)} %param.27) | copy-start | bytes 292
  2.8 31.6 %copy-start.14 = (f32[128]{0:T(128)S(1)}, f32[128]{0:T(128)}, u32[]{:S(2)}) copy-start(f32[128]{0:T(128)} %param.28) | copy-start | bytes 1540
  2.8 49.0 %slice-start.2 = ((s8[6488064]{0:T(1024)(128)(4,1)}), s8[4194304]{0:T(1024)(128)(4,1)S(1)}, s32[]{:S(2)}) async-start(s8[6488064]{0:T(1024)(128)(4,1)} %bitcast.15), calls=%async_computation.5 | async-start | bytes 8388608
  5.0 46.8 %slice-start = ((s8[6488064]{0:T(1024)(128)(4,1)}), s8[4194304]{0:T(1024)(128)(4,1)S(1)}, s32[]{:S(2)}) async-start(s8[6488064]{0:T(1024)(128)(4,1)} %bitcast.12), calls=%async_computation.3 | async-start | bytes 8388608
  5.1 46.8 %slice-start.3 = ((s8[6488064]{0:T(1024)(128)(4,1)}), s8[2293760]{0:T(1024)(128)(4,1)S(1)}, s32[]{:S(2)}) async-start(s8[6488064]{0:T(1024)(128)(4,1)} %bitcast.15), calls=%async_computation.6 | async-start | bytes 4587520
  34.4 17.4 %slice-start.1 = ((s8[6488064]{0:T(1024)(128)(4,1)}), s8[2293760]{0:T(1024)(128)(4,1)S(1)}, s32[]{:S(2)}) async-start(s8[6488064]{0:T(1024)(128)(4,1)} %bitcast.12), calls=%async_computation.4 | async-start | bytes 4587520
  34.4 17.4 %copy-start.1 = (f32[1,24,128,128]{3,2,1,0:T(8,128)S(1)}, f32[1,24,128,128]{3,2,1,0:T(8,128)}, u32[]{:S(2)}) copy-start(f32[1,24,128,128]{3,2,1,0:T(8,128)} %param.18) | copy-start | bytes 4718596
  34.4 17.4 %copy-start.2 = (f32[3072]{0:T(1024)S(1)}, f32[3072]{0:T(1024)}, u32[]{:S(2)}) copy-start(f32[3072]{0:T(1024)} %param.30) | copy-start | bytes 36868
  36.6 30.0 %slice-start.4 = ((s8[6488064]{0:T(1024)(128)(4,1)}), s8[4194304]{0:T(1024)(128)(4,1)S(1)}, s32[]{:S(2)}) async-start(s8[6488064]{0:T(1024)(128)(4,1)} %bitcast.21), calls=%async_computation.7 | async-start | bytes 8388608
  51.9 14.6 %slice-start.5 = ((s8[6488064]{0:T(1024)(128)(4,1)}), s8[2293760]{0:T(1024)(128)(4,1)S(1)}, s32[]{:S(2)}) async-start(s8[6488064]{0:T(1024)(128)(4,1)} %bitcast.21), calls=%async_computation.8 | async-start | bytes 4587520
